TPU v7x, 32 devices: a whole 2x2x4 slice. The times are simulated.
32 devices in a mesh: grp: 2 (over y), sp: 4 (over z), tp: 4 (over x, core).
Axes of the slice: x: 2, y: 2, z: 4, core: 2. Of those that a mesh axis runs over, the one named last changes fastest.
Arguments:
- stream: bfloat16 [2048, 2048], P(('grp', 'sp')), parts along dimension 0, may hold values from -6 to 6
- doc_ids: int32 [2048], P(('grp', 'sp')), parts along dimension 0, may hold values from 0 to 1, never falling along the last dimension, each value on 1 to 768 neighbouring positions
- norm_gain: float32 [2, 2048], replicated, may hold values from 0.1 to 1.9
- query_weight: bfloat16 [2, 2048, 1024], P(None, 'sp', 'tp'), may hold values from -0.125 to 0.125
- key_weight: bfloat16 [2, 2048, 1024], P(None, 'sp', 'tp'), may hold values from -0.125 to 0.125
- value_weight: bfloat16 [2, 2048, 1024], P(None, 'sp', 'tp'), may hold values from -0.125 to 0.125
- out_weight: bfloat16 [2, 1024, 2048], P(None, 'sp', 'tp'), may hold values from -0.75 to 0.75
- query_gain: float32 [2, 64], replicated, may hold values from 0.1 to 1.9
- key_gain: float32 [2, 64], replicated, may hold values from 0.1 to 1.9
- rel_bias: float32 [16, 513], P('tp'), may hold values from -4 to 250
Outputs:
- encoded: bfloat16 [2048, 2048], P(('grp', 'sp')), parts along dimension 0
There are 2 independent parts, one for each index of `grp`. A program takes and returns all parts, laid end to end along the dimension named above; an argument that names none is the same for every part. Nothing has to cross between parts.
Inputs may be any that keep to these rules, and one draw needn't show every extreme that they name: doc_ids never fall along the sequence; each document has at most 768 positions.
All inputs are finite; a program needn't handle non-finite values.
Results may differ from a plain program's by a relative error of at most 0.011.
Values may be sent and summed in bfloat16 or wider, within the bound.
A program may use at most 64 MiB of HBM per device.

v0:
```python
import functools

import jax
import jax.numpy as jnp
from jax import lax
from jax.experimental import pallas as pl
from jax.experimental.pallas import tpu as pltpu
from jax.sharding import PartitionSpec as P

SEG = 64
LEFT = 8
MAXREL = 256
LAYERS = 2


epsilon = 1e-06


def shifted(value, axis, steps):
    count = lax.axis_size(axis)
    initial, last = (max(0, -steps), min(count, count - steps))
    return lax.ppermute(value, axis, [(source, source + steps) for source in range(initial, last)])


def row_norm(values, gain):
    return values * lax.rsqrt(jnp.mean(values * values, axis=-1, keepdims=True) + epsilon) * gain


def bias_table(rel_bias):
    heads_here = rel_bias.shape[0]
    reach = LEFT * SEG
    width = (LEFT + 1) * SEG
    highest = reach + SEG - 1
    reversed_bias = rel_bias[:, ::-1]
    upper_fill = jnp.broadcast_to(rel_bias[:, -1:], (heads_here, highest - MAXREL))
    flat_row = jnp.concatenate([upper_fill, reversed_bias[:, : MAXREL + SEG]], axis=1)
    lines = [
        flat_row[:, SEG - 1 - position : SEG - 1 - position + width] for position in range(SEG)
    ]
    return jnp.stack(lines, axis=1)


def attend(query, ext_keys, ext_values, ext_docs, own_docs, offset, table):
    rows, heads_here, head_size = query.shape
    count = rows // SEG
    width = (LEFT + 1) * SEG
    blocks = query.reshape(count, SEG, heads_here, head_size)
    key_blocks = ext_keys.reshape(count + LEFT, SEG, heads_here, head_size)
    value_blocks = ext_values.reshape(count + LEFT, SEG, heads_here, head_size)
    doc_blocks = ext_docs.reshape(count + LEFT, SEG)
    score_parts = [
        jnp.einsum(
            "nqhd,nkhd->nhqk",
            blocks,
            key_blocks[earlier : earlier + count],
            preferred_element_type=jnp.float32,
        )
        for earlier in range(LEFT + 1)
    ]
    scores = jnp.concatenate(score_parts, axis=-1)
    scores = scores * head_size ** (-0.5) + table[None]
    doc_band = jnp.concatenate(
        [doc_blocks[earlier : earlier + count] for earlier in range(LEFT + 1)], axis=1
    )
    key_pos = (
        offset
        + SEG * jnp.arange(count, dtype=jnp.int32)[:, None]
        - LEFT * SEG
        + jnp.arange(width, dtype=jnp.int32)[None, :]
    )
    allowed = (key_pos >= 0)[:, None, None, :] & (
        doc_band[:, None, None, :] == own_docs.reshape(count, SEG)[:, None, :, None]
    )
    scores = jnp.where(allowed, scores, -1e30)
    peak = jnp.max(scores, axis=-1, keepdims=True)
    expo = jnp.exp(scores - peak)
    weights = (expo / jnp.sum(expo, axis=-1, keepdims=True)).astype(jnp.bfloat16)
    mixed = jnp.zeros((count, SEG, heads_here, head_size), jnp.float32)
    for earlier in range(LEFT + 1):
        part_weights = weights[..., earlier * SEG : (earlier + 1) * SEG]
        mixed = mixed + jnp.einsum(
            "nhqk,nkhd->nqhd",
            part_weights,
            value_blocks[earlier : earlier + count],
            preferred_element_type=jnp.float32,
        )
    return mixed.astype(jnp.bfloat16).reshape(rows, heads_here * head_size)


def on_device(
    stream,
    doc_ids,
    norm_gain,
    query_weight,
    key_weight,
    value_weight,
    out_weight,
    query_gain,
    key_gain,
    rel_bias,
):
    rows = stream.shape[0]
    heads_here = rel_bias.shape[0]
    head_size = query_gain.shape[1]
    local_width = heads_here * head_size
    reach = LEFT * SEG
    depth = -(-reach // rows)
    offset = lax.axis_index("sp") * rows
    col_width = out_weight.shape[2]
    col_start = lax.axis_index("tp") * col_width
    table = bias_table(rel_bias)
    x = stream
    for layer in range(LAYERS):
        widened = x.astype(jnp.float32)
        normed = row_norm(widened, norm_gain[layer]).astype(jnp.bfloat16)
        own_cols = normed
        q_raw = jnp.dot(
            own_cols,
            lax.all_gather(query_weight[layer], "sp", axis=0, tiled=True),
            preferred_element_type=jnp.float32,
        )
        k_raw = jnp.dot(
            normed,
            lax.all_gather(key_weight[layer], "sp", axis=0, tiled=True),
            preferred_element_type=jnp.float32,
        )
        v_raw = jnp.dot(
            normed,
            lax.all_gather(value_weight[layer], "sp", axis=0, tiled=True),
            preferred_element_type=jnp.float32,
        )
        query = row_norm(q_raw.reshape(rows, heads_here, head_size), query_gain[layer]).astype(
            jnp.bfloat16
        )
        keys = row_norm(
            k_raw.reshape(normed.shape[0], heads_here, head_size), key_gain[layer]
        ).astype(jnp.bfloat16)
        values = v_raw.astype(jnp.bfloat16)
        flat_keys = keys.reshape(rows, local_width)
        tail = (flat_keys, values, doc_ids)
        received = [
            shifted((tail[0], tail[1], tail[2]), "sp", distance_back)
            for distance_back in range(depth, 0, -1)
        ]
        ext_keys = jnp.concatenate([item[0] for item in received] + [flat_keys], axis=0)
        ext_values = jnp.concatenate([item[1] for item in received] + [values], axis=0)
        ext_docs = jnp.concatenate([item[2] for item in received] + [doc_ids], axis=0)
        ext_keys = ext_keys.reshape(reach + rows, heads_here, head_size)
        ext_values = ext_values.reshape(reach + rows, heads_here, head_size)
        attended = attend(query, ext_keys, ext_values, ext_docs, doc_ids, offset, table)
        all_heads = lax.all_gather(attended, "tp", axis=1, tiled=True)
        projected = jnp.dot(
            all_heads,
            lax.all_gather(out_weight[layer], "sp", axis=0, tiled=True),
            preferred_element_type=jnp.float32,
        )
        own_cols = lax.dynamic_slice_in_dim(widened, col_start, col_width, 1)
        new_cols = (own_cols + projected).astype(jnp.bfloat16)
        x = lax.all_gather(new_cols, "tp", axis=1, tiled=True)
    return x


MESH = pl.DeviceIdType.MESH
NEG = -1e30


def fused_kernel(
    sizes,
    x_ref,
    docs_ref,
    ngain_ref,
    qw_ref,
    kw_ref,
    vw_ref,
    woin_ref,
    qgain_ref,
    kgain_ref,
    bias_ref,
    out_ref,
    wt_ref,
    xg,
    wq,
    wo,
    docs,
    dcol,
    ag,
    fin,
    bias,
    nb,
    q_s,
    k_s,
    v_s,
    o_s,
    doc_send,
    doc_recv,
    xz_send,
    xz_recv,
    xa_send,
    xa_recv,
    xb_send,
    xb_recv,
    xc_send,
    xc_recv,
    wz_send,
    wz_recv,
    wy_send,
    wy_recv,
    oz_send,
    oz_recv,
    oy_send,
    oy_recv,
    az_send,
    az_recv,
    at_send,
    at_recv,
    fn_send,
    fn_recv,
):
    groups, seqs, tps = sizes
    rows, width = x_ref.shape
    cols = width // tps
    head = qgain_ref.shape[1]
    layers = wt_ref.shape[0]
    depth = bias.shape[0] - 1
    grp = lax.axis_index("grp")
    s = lax.axis_index("sp")
    t = lax.axis_index("tp")
    other_grp = 1 - grp
    core = t + 1 - 2 * lax.rem(t, 2)
    side = lax.rem(t + 2, tps)
    diag = core + 2 - 4 * (core // 2)
    started = []

    def send(src, dst, send_sem, recv_sem, where):
        copy = pltpu.make_async_remote_copy(
            src_ref=src,
            dst_ref=dst,
            send_sem=send_sem,
            recv_sem=recv_sem,
            device_id=where,
            device_id_type=MESH,
        )
        copy.start()
        started.append(copy)
        return copy

    def ahead(o):
        return lax.rem(s + o, seqs)

    def behind(o):
        return lax.rem(s + seqs - o, seqs)

    def block_rows(i):
        return pl.ds(pl.multiple_of(i * rows, rows), rows)

    barrier = pltpu.get_barrier_semaphore()
    partners = [{"sp": ahead(o)} for o in range(1, seqs)]
    partners += [{"tp": core}, {"tp": side}, {"grp": other_grp}]
    for where in partners:
        pl.semaphore_signal(barrier, inc=1, device_id=where, device_id_type=MESH)
    pl.semaphore_wait(barrier, len(partners))

    own_cols = pl.ds(pl.multiple_of(t * cols, cols), cols)
    whalf = wt_ref.shape[2] // 2
    ohalf = woin_ref.shape[1] // 2
    wpart = pl.ds(pl.multiple_of(grp * whalf, whalf), whalf)
    opart = pl.ds(pl.multiple_of(grp * ohalf, ohalf), ohalf)
    hops = list(range(1, seqs))

    doc_c = [
        send(docs_ref, docs.at[s], doc_send.at[o], doc_recv.at[o], {"sp": ahead(o)}) for o in hops
    ]
    def passing(layer, way, k, arriving):
        block = s - k if way == 0 else s + k
        if arriving:
            block = block - 1 if way == 0 else block + 1
        inside = block >= 0 if way == 0 else block < seqs
        return block, inside

    def onward(layer, way, k):
        block, inside = passing(layer, way, k, False)
        open_end = s < seqs - 1 if way == 0 else s > 0
        place = xg.at[layer, t, block_rows(block), :]
        copy = pltpu.make_async_remote_copy(
            src_ref=x_ref.at[:, own_cols] if layer == 0 and k == 0 else place,
            dst_ref=place,
            send_sem=xz_send.at[layer, way, k],
            recv_sem=xz_recv.at[layer, way, k],
            device_id={"sp": s + 1 if way == 0 else s - 1},
            device_id_type=MESH,
        )
        return copy, inside & open_end

    def start_onward(layer, way, k):
        copy, valid = onward(layer, way, k)

        @pl.when(valid)
        def _():
            copy.start()

    def tp_copy(layer, kind, block):
        held = side if kind == 2 else t
        place = xg.at[layer, held, block_rows(block), :]
        send_sem, recv_sem = ((xa_send, xa_recv), (xb_send, xb_recv), (xc_send, xc_recv))[kind]
        return pltpu.make_async_remote_copy(
            src_ref=place,
            dst_ref=place,
            send_sem=send_sem.at[layer, block],
            recv_sem=recv_sem.at[layer, block],
            device_id={"tp": side if kind == 1 else core},
            device_id_type=MESH,
        )

    for way in (0, 1):
        start_onward(0, way, 0)

    def send_qkv(layer):
        return {
            o: send(
                wt_ref.at[layer, ahead(o), wpart, :],
                wq.at[layer, s, wpart, :],
                wz_send.at[layer, o],
                wz_recv.at[layer, o],
                {"sp": ahead(o)},
            )
            for o in hops
        }

    def send_out(layer):
        return {
            o: send(
                woin_ref.at[layer, opart, :],
                wo.at[layer, s, opart, :],
                oz_send.at[layer, o],
                oz_recv.at[layer, o],
                {"sp": ahead(o)},
            )
            for o in hops
        }

    def relay_qkv(layer, flying):
        result = []
        for o in hops:
            flying[o].wait_recv()
            block = wq.at[layer, behind(o), wpart, :]
            result.append(
                send(block, block, wy_send.at[layer, o], wy_recv.at[layer, o], {"grp": other_grp})
            )
        return result

    def relay_out(layer, flying):
        result = []
        for o in hops:
            flying[o].wait_recv()
            block = wo.at[layer, behind(o), opart, :]
            result.append(
                send(block, block, oy_send.at[layer, o], oy_recv.at[layer, o], {"grp": other_grp})
            )
        return result

    for part in range(tps):
        xg[0, part, block_rows(s), :] = x_ref[:, part * cols : (part + 1) * cols]
    for layer in range(layers):
        for which, source in enumerate((qw_ref, kw_ref, vw_ref)):
            turned = jnp.transpose(source[layer])
            for i in range(seqs):
                wt_ref[layer, i, which * head : (which + 1) * head, :] = turned[
                    i * head : (i + 1) * head, :
                ]
        wo[layer, s] = woin_ref[layer]
        wq[layer, s] = wt_ref[layer, s]
    docs[s] = docs_ref[...]
    key_seg = lax.broadcasted_iota(jnp.int32, (rows, rows), 0) // SEG
    query_seg = lax.broadcasted_iota(jnp.int32, (rows, rows), 1) // SEG
    for d in range(depth + 1):
        spread = jnp.broadcast_to(
            bias_ref[pl.ds(s, 1), d * rows : (d + 2) * rows], (rows, 2 * rows)
        )
        rolled = pltpu.roll(spread, 0, 1, stride=1, stride_axis=0)
        gap = query_seg + (d * rows) // SEG - key_seg
        bias[d] = jnp.where((gap >= 0) & (gap <= LEFT), rolled[:, rows:], NEG)
    for copy in doc_c:
        copy.wait_recv()
    for i in range(seqs):
        dcol[i] = jnp.transpose(jnp.broadcast_to(docs[i, 0:1, :], (128, rows)))

    def fan(layer, block):
        tp_copy(layer, 1, block).start()
        tp_copy(layer, 0, block).start()

    def pass_on(layer, block):
        tp_copy(layer, 1, block).wait_recv()
        tp_copy(layer, 2, block).start()

    def spread_tp(layer, own_too):
        fetched = None
        if own_too:
            fan(layer, s)
        for k in range(seqs - 1):
            for way in (0, 1):
                block, inside = passing(layer, way, k, True)

                @pl.when(inside)
                def _(block=block, way=way, k=k):
                    onward(layer, way, k)[0].wait_recv()
                    if k + 1 < seqs - 1:
                        start_onward(layer, way, k + 1)
                    fan(layer, block)

            if k == 0 and own_too:
                fetched = relay_qkv(layer, qkv_fly)
                pass_on(layer, s)
            if k == min(1, seqs - 2) and not own_too:
                flying = send_qkv(layer)
            pass_slots(layer, k - 1)
        out_flying = None
        if own_too:
            out_flying = send_out(layer)
        pass_slots(layer, seqs - 2)
        if not own_too:
            fetched = relay_qkv(layer, flying)
            out_flying = send_out(layer)
        return fetched, out_flying

    def pass_slots(layer, k):
        if k < 0:
            return
        for way in (0, 1):
            block, inside = passing(layer, way, k, True)

            @pl.when(inside)
            def _(block=block):
                pass_on(layer, block)

    def nth(v):
        orders = [
            sorted((b for b in range(seqs) if b != c), key=lambda b: abs(b - c))
            for c in range(seqs)
        ]
        block = orders[0][v - 1]
        for c in range(1, seqs):
            block = jnp.where(s == c, orders[c][v - 1], block)
        return block

    def project(layer, i):
        total = jnp.zeros((rows, 1), jnp.float32)
        for part in range(tps):
            piece = xg[layer, part, block_rows(i), :].astype(jnp.float32)
            total = total + jnp.sum(piece * piece, axis=1, keepdims=True)
        factor = lax.rsqrt(total * (1.0 / width) + epsilon)
        for part in range(tps):
            piece = xg[layer, part, block_rows(i), :].astype(jnp.float32)
            gain = ngain_ref[layer : layer + 1, part * cols : (part + 1) * cols]
            nb[:, part * cols : (part + 1) * cols] = (piece * factor * gain).astype(jnp.bfloat16)
        span = width // seqs
        raw = jnp.zeros((3 * head, rows), jnp.float32)
        for part in range(seqs):
            raw = raw + lax.dot_general(
                wq[layer, part],
                nb[:, part * span : (part + 1) * span],
                (((1,), (1,)), ((), ())),
                preferred_element_type=jnp.float32,
            )

        def normal(value, gain):
            mean = jnp.mean(value * value, axis=0, keepdims=True)
            column = jnp.transpose(jnp.broadcast_to(gain, (128, head)))[:, 0:1]
            return value * lax.rsqrt(mean + epsilon) * column

        q_s[i] = (normal(raw[:head], qgain_ref[layer : layer + 1, :]) * head ** (-0.5)).astype(jnp.bfloat16)
        k_s[i] = jnp.transpose(normal(raw[head : 2 * head], kgain_ref[layer : layer + 1, :])).astype(jnp.bfloat16)
        v_s[i] = raw[2 * head :].astype(jnp.bfloat16)

    def attention():
        for j in range(seqs):
            pieces = []
            for i in range(max(0, j - depth), j + 1):
                score = jnp.dot(k_s[i], q_s[j], preferred_element_type=jnp.float32)
                same = dcol[i][:, 0:1] == docs[j, 0:1, :]
                pieces.append((i, jnp.where(same, score + bias[j - i], NEG)))
            peak = pieces[0][1].max(axis=0, keepdims=True)
            for _, piece in pieces[1:]:
                peak = jnp.maximum(peak, piece.max(axis=0, keepdims=True))
            mass = jnp.zeros((1, rows), jnp.float32)
            mixed = jnp.zeros((head, rows), jnp.float32)
            for i, piece in pieces:
                expo = jnp.exp(piece - peak)
                mass = mass + jnp.sum(expo, axis=0, keepdims=True)
                mixed = mixed + jnp.dot(
                    v_s[i], expo.astype(jnp.bfloat16), preferred_element_type=jnp.float32
                )
            o_s[lax.rem(j, seqs)] = (mixed / mass).astype(jnp.bfloat16)

    for layer in range(layers):
        last = layer == layers - 1
        project_ready, out_fly = spread_tp(layer, layer > 0)
        for copy in project_ready:
            copy.wait_recv()
        for v in range(seqs):
            block = nth(v) if v else s
            if v or layer > 0:
                tp_copy(layer, 0, block).wait_recv()
                tp_copy(layer, 2, block).wait_recv()
            project(layer, block)
        if layer > 0:
            for copy in outgoing:
                copy.wait_send()
            started[:] = [copy for copy in started if all(copy is not old for old in outgoing)]
        attention()
        outgoing = [
            send(
                o_s.at[ahead(o)],
                ag.at[layer, t, s],
                az_send.at[layer, o],
                az_recv.at[layer, o],
                {"sp": ahead(o)},
            )
            for o in hops
        ]
        if not last:
            qkv_fly = send_qkv(layer + 1)
        ag[layer, t, s] = o_s[s]
        out_ready = relay_out(layer, out_fly)
        for copy in outgoing:
            copy.wait_recv()
        block = ag.at[layer, t]
        across = send(block, block, at_send.at[layer, 0], at_recv.at[layer, 0], {"tp": side})
        beside = send(block, block, at_send.at[layer, 1], at_recv.at[layer, 1], {"tp": core})
        across.wait_recv()
        block = ag.at[layer, side]
        corner = send(block, block, at_send.at[layer, 2], at_recv.at[layer, 2], {"tp": core})
        for copy in out_ready:
            copy.wait_recv()
        beside.wait_recv()
        corner.wait_recv()
        heads_all = ag[layer].reshape(tps * seqs * head, rows)
        weight = wo[layer].reshape(-1, cols)
        product = lax.dot_general(
            heads_all,
            weight,
            (((0,), (0,)), ((), ())),
            preferred_element_type=jnp.float32,
        )
        kept = xg[layer, t, block_rows(s), :].astype(jnp.float32)
        fresh = (kept + product).astype(jnp.bfloat16)
        if not last:
            xg[layer + 1, t, block_rows(s), :] = fresh
            for way in (0, 1):
                start_onward(layer + 1, way, 0)
        else:
            fin[t] = fresh
            cuts = fn_send.shape[0]
            tall = rows // cuts
            crossing, beside = [], []
            for c in range(cuts):
                part = fin.at[t, pl.ds(c * tall, tall), :]
                crossing.append(send(part, part, fn_send.at[c, 0], fn_recv.at[c, 0], {"tp": side}))
                beside.append(send(part, part, fn_send.at[c, 1], fn_recv.at[c, 1], {"tp": core}))
            for c in range(cuts):
                crossing[c].wait_recv()
                part = fin.at[side, pl.ds(c * tall, tall), :]
                beside.append(send(part, part, fn_send.at[c, 2], fn_recv.at[c, 2], {"tp": core}))
            for copy in beside:
                copy.wait_recv()
            for part in range(tps):
                out_ref[:, part * cols : (part + 1) * cols] = fin[part]
    for copy in started:
        copy.wait_send()
    for layer in range(layers):
        for o in range(1 if layer == 0 else 0, seqs):
            for kind in range(3):
                tp_copy(layer, kind, ahead(o)).wait_send()
        for way in (0, 1):
            for k in range(seqs - 1):
                copy, valid = onward(layer, way, k)

                @pl.when(valid)
                def _(copy=copy):
                    copy.wait_send()


def fused_device(
    sizes,
    stream,
    doc_ids,
    norm_gain,
    query_weight,
    key_weight,
    value_weight,
    out_weight,
    query_gain,
    key_gain,
    rel_bias,
):
    groups, seqs, tps = sizes
    rows, width = stream.shape
    cols = width // tps
    layers, deep, _ = query_weight.shape
    head = query_gain.shape[1]
    depth = -(-LEFT * SEG // rows)

    padded = jnp.pad(
        rel_bias, ((0, 0), (0, (depth + 2) * rows - rel_bias.shape[1])), mode="edge"
    )
    docs8 = jnp.broadcast_to(doc_ids.astype(jnp.float32)[None], (8, rows))
    dma = pltpu.SemaphoreType.DMA
    bf16 = jnp.bfloat16
    scratch = [
        pltpu.VMEM((layers, seqs, 3 * head, deep), bf16),
        pltpu.VMEM((layers, tps, seqs * rows, cols), bf16),
        pltpu.VMEM((layers, seqs, 3 * head, deep), bf16),
        pltpu.VMEM((layers, seqs) + out_weight.shape[1:], bf16),
        pltpu.VMEM((seqs, 8, rows), jnp.float32),
        pltpu.VMEM((seqs, rows, 128), jnp.float32),
        pltpu.VMEM((layers, tps, seqs, head, rows), bf16),
        pltpu.VMEM((tps, rows, cols), bf16),
        pltpu.VMEM((depth + 1, rows, rows), jnp.float32),
        pltpu.VMEM((rows, width), bf16),
        pltpu.VMEM((seqs, head, rows), bf16),
        pltpu.VMEM((seqs, rows, head), bf16),
        pltpu.VMEM((seqs, head, rows), bf16),
        pltpu.VMEM((seqs, head, rows), bf16),
    ]
    scratch += [dma((seqs,))] * 2 + [dma((layers, 2, seqs))] * 2 + [dma((layers, seqs))] * 14
    scratch += [dma((layers, seqs))] * 2 + [dma((layers, 3))] * 2 + [dma((2, 3))] * 2
    return pl.pallas_call(
        functools.partial(fused_kernel, sizes),
        name="fused_layers",
        out_shape=jax.ShapeDtypeStruct((rows, width), bf16),
        in_specs=[pl.BlockSpec(memory_space=pltpu.VMEM)] * 10,
        out_specs=pl.BlockSpec(memory_space=pltpu.VMEM),
        scratch_shapes=scratch,
        compiler_params=pltpu.CompilerParams(
            collective_id=0, has_side_effects=True, vmem_limit_bytes=60 * 1024 * 1024
        ),
    )(
        stream,
        docs8,
        norm_gain,
        query_weight,
        key_weight,
        value_weight,
        out_weight,
        query_gain,
        key_gain,
        padded,
    )


def solution(mesh):
    placed = (
        P(("grp", "sp"), None),
        P(("grp", "sp")),
        P(),
        P(None, "sp", "tp"),
        P(None, "sp", "tp"),
        P(None, "sp", "tp"),
        P(None, "sp", "tp"),
        P(),
        P(),
        P("tp", None),
    )
    sizes = tuple(mesh.shape[axis] for axis in ("grp", "sp", "tp"))

    def body(*args):
        one_head_each = args[-1].shape[0] == sizes[1]
        fits = sizes[0] == 2 and sizes[2] == 4 and args[0].shape[0] == MAXREL
        if one_head_each and fits:
            return fused_device(sizes, *args)
        return on_device(*args)

    return jax.shard_map(
        body, mesh=mesh, in_specs=placed, out_specs=P(("grp", "sp"), None), check_vma=False
    )
```

profile of v0, /device:TPU:0, one launch (start us, length us, event | category | flops | bytes accessed | tf_op | source)
XLA Modules:
  0.0 120.2 jit_solution(17652810274793033667)
XLA Ops:
  0.0 0.0 copy-start.1
  0.0 0.8 slice_reduce_fusion
  0.8 0.0 copy-done.1
  0.8 0.0 copy-start
  0.8 0.6 broadcast_in_dim.4.docs_ref
  1.4 0.1 reshape.6
  1.5 0.0 copy-done
  1.5 0.7 pad_maximum_fusion.bias_ref
  2.2 115.7 %fused_layers.1 = bf16[256,2048]{1,0:T(8,128)(2,1)} custom-call(bf16[256,2048]{1,0:T(8,128)(2,1)} %x_ref.1, f32[8,256]{1,0:T(8,128)} %broadcast_in_dim.4.docs_ref, f32[2,2048]{1,0:T(2,128)} %ngain_ref.1, bf16[2,512,256]{2,1,0:T(8,128)(2,1)} %qw_ref.1, bf16[2,512,256]{2,1,0:T(8,128)(2,1)} %kw_ref.1, bf16[2,512,256]{2,1,0:T(8,128)(2,1)} %vw_ref.1, ...), custom_call_target="tpu_custom_call" | custom-call | tf_op jit(solution)/shard_map/fused_layers/pallas_call | solution.py:626
  117.9 2.3 %copy.12 = bf16[256,2048]{1,0:T(8,128)(2,1)} copy(bf16[256,2048]{1,0:T(8,128)(2,1)} %fused_layers.1) | data formatting | bytes 2097152
  (1 shorter events, 0.0 us)
Async XLA Ops:
  0.0 0.8 copy-start.1
  0.8 0.7 copy-start
where the time goes:
time: 120 us
  Pallas kernels  116 us (97%)
  local copies, waits for them, and re-layouts  3.8 us (3%)
    pallas_call x1, Pallas kernels, fused_device(): pl.pallas_call(functools.partial(fused_kernel, sizes), name='fused_layers...  116 us

commit v1 on v0

--- a/solution.py
+++ b/solution.py
@@ -183,6 +183,7 @@
     wo,
     docs,
     dcol,
+    mids,
     ag,
     fin,
     bias,
@@ -195,20 +196,28 @@
     doc_recv,
     xz_send,
     xz_recv,
-    xa_send,
-    xa_recv,
-    xb_send,
-    xb_recv,
-    xc_send,
-    xc_recv,
+    xt_send,
+    xt_recv,
     wz_send,
     wz_recv,
     wy_send,
     wy_recv,
     oz_send,
     oz_recv,
+    ox_send,
+    ox_recv,
     oy_send,
     oy_recv,
+    op_send,
+    op_recv,
+    mz_send,
+    mz_recv,
+    mx_send,
+    mx_recv,
+    mc_send,
+    mc_recv,
+    nc_send,
+    nc_recv,
     az_send,
     az_recv,
     at_send,
@@ -228,15 +237,14 @@
     other_grp = 1 - grp
     core = t + 1 - 2 * lax.rem(t, 2)
     side = lax.rem(t + 2, tps)
-    diag = core + 2 - 4 * (core // 2)
     started = []
 
-    def send(src, dst, send_sem, recv_sem, where):
+    def send(src, dst, sems, index, where):
         copy = pltpu.make_async_remote_copy(
             src_ref=src,
             dst_ref=dst,
-            send_sem=send_sem,
-            recv_sem=recv_sem,
+            send_sem=sems[0].at[index],
+            recv_sem=sems[1].at[index],
             device_id=where,
             device_id_type=MESH,
         )
@@ -267,72 +275,72 @@
     opart = pl.ds(pl.multiple_of(grp * ohalf, ohalf), ohalf)
     hops = list(range(1, seqs))
 
-    doc_c = [
-        send(docs_ref, docs.at[s], doc_send.at[o], doc_recv.at[o], {"sp": ahead(o)}) for o in hops
-    ]
-    def passing(layer, way, k, arriving):
+    def passing(way, k, arriving):
         block = s - k if way == 0 else s + k
         if arriving:
             block = block - 1 if way == 0 else block + 1
         inside = block >= 0 if way == 0 else block < seqs
         return block, inside
 
-    def onward(layer, way, k):
-        block, inside = passing(layer, way, k, False)
+    def onward(way, k):
+        block, inside = passing(way, k, False)
         open_end = s < seqs - 1 if way == 0 else s > 0
-        place = xg.at[layer, t, block_rows(block), :]
+        place = xg.at[0, t, block_rows(block), :]
         copy = pltpu.make_async_remote_copy(
-            src_ref=x_ref.at[:, own_cols] if layer == 0 and k == 0 else place,
+            src_ref=x_ref.at[:, own_cols] if k == 0 else place,
             dst_ref=place,
-            send_sem=xz_send.at[layer, way, k],
-            recv_sem=xz_recv.at[layer, way, k],
+            send_sem=xz_send.at[way, k],
+            recv_sem=xz_recv.at[way, k],
             device_id={"sp": s + 1 if way == 0 else s - 1},
             device_id_type=MESH,
         )
         return copy, inside & open_end
 
-    def start_onward(layer, way, k):
-        copy, valid = onward(layer, way, k)
+    def start_onward(way, k):
+        copy, valid = onward(way, k)
 
         @pl.when(valid)
         def _():
             copy.start()
 
-    def tp_copy(layer, kind, block):
+    def tp_copy(kind, block):
         held = side if kind == 2 else t
-        place = xg.at[layer, held, block_rows(block), :]
-        send_sem, recv_sem = ((xa_send, xa_recv), (xb_send, xb_recv), (xc_send, xc_recv))[kind]
+        place = xg.at[0, held, block_rows(block), :]
         return pltpu.make_async_remote_copy(
             src_ref=place,
             dst_ref=place,
-            send_sem=send_sem.at[layer, block],
-            recv_sem=recv_sem.at[layer, block],
+            send_sem=xt_send.at[kind, block],
+            recv_sem=xt_recv.at[kind, block],
             device_id={"tp": side if kind == 1 else core},
             device_id_type=MESH,
         )
 
+    def fan(block):
+        tp_copy(1, block).start()
+        tp_copy(0, block).start()
+
+    def pass_slots(k):
+        for way in (0, 1):
+            block, inside = passing(way, k, True)
+
+            @pl.when(inside)
+            def _(block=block):
+                tp_copy(1, block).wait_recv()
+                tp_copy(2, block).start()
+
     for way in (0, 1):
-        start_onward(0, way, 0)
+        start_onward(way, 0)
+    doc_c = [
+        send(docs_ref, docs.at[s], (doc_send, doc_recv), o, {"sp": ahead(o)}) for o in hops
+    ]
 
     def send_qkv(layer):
         return {
             o: send(
                 wt_ref.at[layer, ahead(o), wpart, :],
                 wq.at[layer, s, wpart, :],
-                wz_send.at[layer, o],
-                wz_recv.at[layer, o],
-                {"sp": ahead(o)},
-            )
-            for o in hops
-        }
-
-    def send_out(layer):
-        return {
-            o: send(
-                woin_ref.at[layer, opart, :],
-                wo.at[layer, s, opart, :],
-                oz_send.at[layer, o],
-                oz_recv.at[layer, o],
+                (wz_send, wz_recv),
+                (layer, o),
                 {"sp": ahead(o)},
             )
             for o in hops
@@ -343,32 +351,57 @@
         for o in hops:
             flying[o].wait_recv()
             block = wq.at[layer, behind(o), wpart, :]
-            result.append(
-                send(block, block, wy_send.at[layer, o], wy_recv.at[layer, o], {"grp": other_grp})
+            result.append(send(block, block, (wy_send, wy_recv), (layer, o), {"grp": other_grp}))
+        return result
+
+    def send_out(layer):
+        flying = {
+            o: send(
+                woin_ref.at[layer, opart, :],
+                wo.at[layer, t, s, opart, :],
+                (oz_send, oz_recv),
+                (layer, o),
+                {"sp": ahead(o)},
             )
-        return result
+            for o in hops
+        }
+        whole = send(
+            woin_ref.at[layer], wo.at[layer, t, s], (ox_send, ox_recv), (layer, 0), {"tp": side}
+        )
+        return flying, whole
 
     def relay_out(layer, flying):
-        result = []
+        across, over = {}, []
         for o in hops:
             flying[o].wait_recv()
-            block = wo.at[layer, behind(o), opart, :]
-            result.append(
-                send(block, block, oy_send.at[layer, o], oy_recv.at[layer, o], {"grp": other_grp})
-            )
-        return result
-
-    for part in range(tps):
-        xg[0, part, block_rows(s), :] = x_ref[:, part * cols : (part + 1) * cols]
-    for layer in range(layers):
+            block = wo.at[layer, t, behind(o), opart, :]
+            across[o] = send(block, block, (ox_send, ox_recv), (layer, o), {"tp": side})
+            over.append(send(block, block, (oy_send, oy_recv), (layer, o), {"grp": other_grp}))
+        return across, over
+
+    def relay_side(layer, across, over):
+        for o in hops:
+            across[o].wait_recv()
+            block = wo.at[layer, side, behind(o), opart, :]
+            over.append(send(block, block, (op_send, op_recv), (layer, o), {"grp": other_grp}))
+
+    def turn(layer):
         for which, source in enumerate((qw_ref, kw_ref, vw_ref)):
             turned = jnp.transpose(source[layer])
             for i in range(seqs):
                 wt_ref[layer, i, which * head : (which + 1) * head, :] = turned[
                     i * head : (i + 1) * head, :
                 ]
-        wo[layer, s] = woin_ref[layer]
         wq[layer, s] = wt_ref[layer, s]
+
+    turn(0)
+    qkv_fly = send_qkv(0)
+    for part in range(tps):
+        xg[0, part, block_rows(s), :] = x_ref[:, part * cols : (part + 1) * cols]
+    for layer in range(1, layers):
+        turn(layer)
+    for layer in range(layers):
+        wo[layer, t, s] = woin_ref[layer]
     docs[s] = docs_ref[...]
     key_seg = lax.broadcasted_iota(jnp.int32, (rows, rows), 0) // SEG
     query_seg = lax.broadcasted_iota(jnp.int32, (rows, rows), 1) // SEG
@@ -384,53 +417,23 @@
     for i in range(seqs):
         dcol[i] = jnp.transpose(jnp.broadcast_to(docs[i, 0:1, :], (128, rows)))
 
-    def fan(layer, block):
-        tp_copy(layer, 1, block).start()
-        tp_copy(layer, 0, block).start()
-
-    def pass_on(layer, block):
-        tp_copy(layer, 1, block).wait_recv()
-        tp_copy(layer, 2, block).start()
-
-    def spread_tp(layer, own_too):
-        fetched = None
-        if own_too:
-            fan(layer, s)
-        for k in range(seqs - 1):
-            for way in (0, 1):
-                block, inside = passing(layer, way, k, True)
-
-                @pl.when(inside)
-                def _(block=block, way=way, k=k):
-                    onward(layer, way, k)[0].wait_recv()
-                    if k + 1 < seqs - 1:
-                        start_onward(layer, way, k + 1)
-                    fan(layer, block)
-
-            if k == 0 and own_too:
-                fetched = relay_qkv(layer, qkv_fly)
-                pass_on(layer, s)
-            if k == min(1, seqs - 2) and not own_too:
-                flying = send_qkv(layer)
-            pass_slots(layer, k - 1)
-        out_flying = None
-        if own_too:
-            out_flying = send_out(layer)
-        pass_slots(layer, seqs - 2)
-        if not own_too:
-            fetched = relay_qkv(layer, flying)
-            out_flying = send_out(layer)
-        return fetched, out_flying
-
-    def pass_slots(layer, k):
-        if k < 0:
-            return
+    for k in range(seqs - 1):
         for way in (0, 1):
-            block, inside = passing(layer, way, k, True)
+            block, inside = passing(way, k, True)
 
             @pl.when(inside)
-            def _(block=block):
-                pass_on(layer, block)
+            def _(block=block, way=way, k=k):
+                onward(way, k)[0].wait_recv()
+                if k + 1 < seqs - 1:
+                    start_onward(way, k + 1)
+                fan(block)
+
+        if k == 0:
+            qkv_ready = relay_qkv(0, qkv_fly)
+        else:
+            pass_slots(k - 1)
+    out_fly, out_whole = send_out(0)
+    pass_slots(seqs - 2)
 
     def nth(v):
         orders = [
@@ -471,112 +474,150 @@
         k_s[i] = jnp.transpose(normal(raw[head : 2 * head], kgain_ref[layer : layer + 1, :])).astype(jnp.bfloat16)
         v_s[i] = raw[2 * head :].astype(jnp.bfloat16)
 
-    def attention():
-        for j in range(seqs):
-            pieces = []
-            for i in range(max(0, j - depth), j + 1):
-                score = jnp.dot(k_s[i], q_s[j], preferred_element_type=jnp.float32)
-                same = dcol[i][:, 0:1] == docs[j, 0:1, :]
-                pieces.append((i, jnp.where(same, score + bias[j - i], NEG)))
-            peak = pieces[0][1].max(axis=0, keepdims=True)
-            for _, piece in pieces[1:]:
-                peak = jnp.maximum(peak, piece.max(axis=0, keepdims=True))
-            mass = jnp.zeros((1, rows), jnp.float32)
-            mixed = jnp.zeros((head, rows), jnp.float32)
-            for i, piece in pieces:
-                expo = jnp.exp(piece - peak)
-                mass = mass + jnp.sum(expo, axis=0, keepdims=True)
-                mixed = mixed + jnp.dot(
-                    v_s[i], expo.astype(jnp.bfloat16), preferred_element_type=jnp.float32
-                )
-            o_s[lax.rem(j, seqs)] = (mixed / mass).astype(jnp.bfloat16)
-
-    for layer in range(layers):
-        last = layer == layers - 1
-        project_ready, out_fly = spread_tp(layer, layer > 0)
-        for copy in project_ready:
-            copy.wait_recv()
-        for v in range(seqs):
-            block = nth(v) if v else s
-            if v or layer > 0:
-                tp_copy(layer, 0, block).wait_recv()
-                tp_copy(layer, 2, block).wait_recv()
-            project(layer, block)
-        if layer > 0:
-            for copy in outgoing:
-                copy.wait_send()
-            started[:] = [copy for copy in started if all(copy is not old for old in outgoing)]
-        attention()
-        outgoing = [
-            send(
-                o_s.at[ahead(o)],
-                ag.at[layer, t, s],
-                az_send.at[layer, o],
-                az_recv.at[layer, o],
-                {"sp": ahead(o)},
+    def attend_block(j):
+        pieces = []
+        for i in range(max(0, j - depth), j + 1):
+            score = jnp.dot(k_s[i], q_s[j], preferred_element_type=jnp.float32)
+            same = dcol[i][:, 0:1] == docs[j, 0:1, :]
+            pieces.append((i, jnp.where(same, score + bias[j - i], NEG)))
+        peak = pieces[0][1].max(axis=0, keepdims=True)
+        for _, piece in pieces[1:]:
+            peak = jnp.maximum(peak, piece.max(axis=0, keepdims=True))
+        mass = jnp.zeros((1, rows), jnp.float32)
+        mixed = jnp.zeros((head, rows), jnp.float32)
+        for i, piece in pieces:
+            expo = jnp.exp(piece - peak)
+            mass = mass + jnp.sum(expo, axis=0, keepdims=True)
+            mixed = mixed + jnp.dot(
+                v_s[i], expo.astype(jnp.bfloat16), preferred_element_type=jnp.float32
             )
-            for o in hops
-        ]
-        if not last:
-            qkv_fly = send_qkv(layer + 1)
-        ag[layer, t, s] = o_s[s]
-        out_ready = relay_out(layer, out_fly)
-        for copy in outgoing:
-            copy.wait_recv()
-        block = ag.at[layer, t]
-        across = send(block, block, at_send.at[layer, 0], at_recv.at[layer, 0], {"tp": side})
-        beside = send(block, block, at_send.at[layer, 1], at_recv.at[layer, 1], {"tp": core})
-        across.wait_recv()
-        block = ag.at[layer, side]
-        corner = send(block, block, at_send.at[layer, 2], at_recv.at[layer, 2], {"tp": core})
-        for copy in out_ready:
-            copy.wait_recv()
-        beside.wait_recv()
-        corner.wait_recv()
-        heads_all = ag[layer].reshape(tps * seqs * head, rows)
-        weight = wo[layer].reshape(-1, cols)
-        product = lax.dot_general(
+        return (mixed / mass).astype(jnp.bfloat16)
+
+    def out_product(layer, heads_all, held):
+        return lax.dot_general(
             heads_all,
-            weight,
+            wo[layer, held].reshape(-1, cols),
             (((0,), (0,)), ((), ())),
             preferred_element_type=jnp.float32,
         )
-        kept = xg[layer, t, block_rows(s), :].astype(jnp.float32)
-        fresh = (kept + product).astype(jnp.bfloat16)
-        if not last:
-            xg[layer + 1, t, block_rows(s), :] = fresh
-            for way in (0, 1):
-                start_onward(layer + 1, way, 0)
-        else:
-            fin[t] = fresh
-            cuts = fn_send.shape[0]
-            tall = rows // cuts
-            crossing, beside = [], []
-            for c in range(cuts):
-                part = fin.at[t, pl.ds(c * tall, tall), :]
-                crossing.append(send(part, part, fn_send.at[c, 0], fn_recv.at[c, 0], {"tp": side}))
-                beside.append(send(part, part, fn_send.at[c, 1], fn_recv.at[c, 1], {"tp": core}))
-            for c in range(cuts):
-                crossing[c].wait_recv()
-                part = fin.at[side, pl.ds(c * tall, tall), :]
-                beside.append(send(part, part, fn_send.at[c, 2], fn_recv.at[c, 2], {"tp": core}))
-            for copy in beside:
-                copy.wait_recv()
-            for part in range(tps):
-                out_ref[:, part * cols : (part + 1) * cols] = fin[part]
+
+    for copy in qkv_ready:
+        copy.wait_recv()
+    for v in range(seqs):
+        block = nth(v) if v else s
+        if v:
+            tp_copy(0, block).wait_recv()
+            tp_copy(2, block).wait_recv()
+        project(0, block)
+
+    mid_z, mid_x, mid_c, new_c = {}, {}, {}, {}
+    for j in range(seqs):
+        mids[j, t, s] = attend_block(j)
+        place = mids.at[j, t, s]
+        for o in hops:
+            mid_z[j, o] = send(place, place, (mz_send, mz_recv), (j, o), {"sp": ahead(o)})
+        mid_x[j, 0] = send(place, place, (mx_send, mx_recv), (j, 0), {"tp": side})
+    out_across, out_over = relay_out(0, out_fly)
+    qkv_fly = send_qkv(1)
+
+    def mid_first(j):
+        for o in hops:
+            mid_z[j, o].wait_recv()
+            place = mids.at[j, t, behind(o)]
+            mid_x[j, o] = send(place, place, (mx_send, mx_recv), (j, o), {"tp": side})
+        place = mids.at[j, t]
+        mid_c[j, 0] = send(place, place, (mc_send, mc_recv), (j, 0), {"tp": core})
+
+    def mid_second(j):
+        for o in range(seqs):
+            mid_x[j, o].wait_recv()
+        place = mids.at[j, side]
+        mid_c[j, 1] = send(place, place, (mc_send, mc_recv), (j, 1), {"tp": core})
+
+    def mid_third(j):
+        for half in range(2):
+            mid_c[j, half].wait_recv()
+        heads_all = mids[j].reshape(tps * seqs * head, rows)
+        for half, held in enumerate((t, side)):
+            kept = xg[0, held, block_rows(j), :].astype(jnp.float32)
+            place = xg.at[1, held, block_rows(j), :]
+            place[...] = (kept + out_product(0, heads_all, held)).astype(jnp.bfloat16)
+            new_c[j, half] = send(place, place, (nc_send, nc_recv), (j, half), {"tp": core})
+
+    def mid_fourth(j):
+        for half in range(2):
+            new_c[j, half].wait_recv()
+        project(1, j)
+
+    mid_first(0)
+    mid_first(1)
+    relay_side(0, out_across, out_over)
+    mid_second(0)
+    mid_first(2)
+    mid_second(1)
+    mid_first(3)
+    mid_second(2)
+    qkv_ready = relay_qkv(1, qkv_fly)
+    out_whole.wait_recv()
+    for copy in out_over:
+        copy.wait_recv()
+    mid_third(0)
+    mid_second(3)
+    out_fly, out_whole = send_out(1)
+    mid_third(1)
+    for copy in qkv_ready:
+        copy.wait_recv()
+    mid_fourth(0)
+    mid_third(2)
+    mid_fourth(1)
+    mid_third(3)
+    mid_fourth(2)
+    out_across, out_over = relay_out(1, out_fly)
+    mid_fourth(3)
+
+    for j in range(seqs):
+        o_s[j] = attend_block(j)
+    outgoing = [
+        send(o_s.at[ahead(o)], ag.at[t, s], (az_send, az_recv), o, {"sp": ahead(o)}) for o in hops
+    ]
+    ag[t, s] = o_s[s]
+    relay_side(1, out_across, out_over)
+    for copy in outgoing:
+        copy.wait_recv()
+    block = ag.at[t]
+    across = send(block, block, (at_send, at_recv), 0, {"tp": side})
+    beside = send(block, block, (at_send, at_recv), 1, {"tp": core})
+    out_whole.wait_recv()
+    for copy in out_over:
+        copy.wait_recv()
+    across.wait_recv()
+    block = ag.at[side]
+    corner = send(block, block, (at_send, at_recv), 2, {"tp": core})
+    beside.wait_recv()
+    corner.wait_recv()
+    heads_all = ag[...].reshape(tps * seqs * head, rows)
+    last = []
+    for half, held in enumerate((t, side)):
+        kept = xg[1, held, block_rows(s), :].astype(jnp.float32)
+        fin[held] = (kept + out_product(1, heads_all, held)).astype(jnp.bfloat16)
+        place = fin.at[held]
+        last.append(send(place, place, (fn_send, fn_recv), half, {"tp": core}))
+    for copy in last:
+        copy.wait_recv()
+    for part in range(tps):
+        out_ref[:, part * cols : (part + 1) * cols] = fin[part]
     for copy in started:
         copy.wait_send()
-    for layer in range(layers):
-        for o in range(1 if layer == 0 else 0, seqs):
-            for kind in range(3):
-                tp_copy(layer, kind, ahead(o)).wait_send()
-        for way in (0, 1):
-            for k in range(seqs - 1):
-                copy, valid = onward(layer, way, k)
-
-                @pl.when(valid)
-                def _(copy=copy):
-                    copy.wait_send()
+    for o in hops:
+        for kind in range(3):
+            tp_copy(kind, ahead(o)).wait_send()
+    for way in (0, 1):
+        for k in range(seqs - 1):
+            copy, valid = onward(way, k)
+
+            @pl.when(valid)
+            def _(copy=copy):
+                copy.wait_send()
 
 
 def fused_device(
@@ -609,10 +650,11 @@
         pltpu.VMEM((layers, seqs, 3 * head, deep), bf16),
         pltpu.VMEM((layers, tps, seqs * rows, cols), bf16),
         pltpu.VMEM((layers, seqs, 3 * head, deep), bf16),
-        pltpu.VMEM((layers, seqs) + out_weight.shape[1:], bf16),
+        pltpu.VMEM((layers, tps, seqs) + out_weight.shape[1:], bf16),
         pltpu.VMEM((seqs, 8, rows), jnp.float32),
         pltpu.VMEM((seqs, rows, 128), jnp.float32),
-        pltpu.VMEM((layers, tps, seqs, head, rows), bf16),
+        pltpu.VMEM((seqs, tps, seqs, head, rows), bf16),
+        pltpu.VMEM((tps, seqs, head, rows), bf16),
         pltpu.VMEM((tps, rows, cols), bf16),
         pltpu.VMEM((depth + 1, rows, rows), jnp.float32),
         pltpu.VMEM((rows, width), bf16),
@@ -621,8 +663,25 @@
         pltpu.VMEM((seqs, head, rows), bf16),
         pltpu.VMEM((seqs, head, rows), bf16),
     ]
-    scratch += [dma((seqs,))] * 2 + [dma((layers, 2, seqs))] * 2 + [dma((layers, seqs))] * 14
-    scratch += [dma((layers, seqs))] * 2 + [dma((layers, 3))] * 2 + [dma((2, 3))] * 2
+    pairs = [
+        (seqs,),
+        (2, seqs),
+        (3, seqs),
+        (layers, seqs),
+        (layers, seqs),
+        (layers, seqs),
+        (layers, seqs),
+        (layers, seqs),
+        (layers, seqs),
+        (seqs, seqs),
+        (seqs, seqs),
+        (seqs, 2),
+        (seqs, 2),
+        (seqs,),
+        (3,),
+        (2,),
+    ]
+    scratch += [dma(shape) for shape in pairs for _ in range(2)]
     return pl.pallas_call(
         functools.partial(fused_kernel, sizes),
         name="fused_layers",

time: 120 us -> 108 us (0.900)
  Pallas kernels: 116 us -> 103 us
    pallas_call x1, Pallas kernels: 116 us -> 103 us  [fused_device(): pl.pallas_call(functools.partial(fused_kernel, sizes), name='fused_layers...]
where the time goes in v1:
time: 108 us
  Pallas kernels  103 us (95%)
  local copies, waits for them, and re-layouts  3.8 us (4%)
    pallas_call x1, Pallas kernels, fused_device(): pl.pallas_call(functools.partial(fused_kernel, sizes), name='fused_layers...  103 us
    unnamed x5, local copies, waits for them, and re-layouts  2.33 us

profile of v1, /device:TPU:0, one launch (start us, length us, event | category | flops | bytes accessed | tf_op | source)
XLA Modules:
  0.0 107.9 jit_solution(6221479071971407615)
XLA Ops:
  0.0 0.0 copy-start.1
  0.0 0.8 slice_reduce_fusion
  0.8 0.0 copy-done.1
  0.8 0.0 copy-start
  0.8 0.6 broadcast_in_dim.4.docs_ref
  1.4 0.1 reshape.6
  1.5 0.0 copy-done
  1.5 0.7 pad_maximum_fusion.bias_ref
  2.2 103.4 %fused_layers.1 = bf16[256,2048]{1,0:T(8,128)(2,1)} custom-call(bf16[256,2048]{1,0:T(8,128)(2,1)} %x_ref.1, f32[8,256]{1,0:T(8,128)} %broadcast_in_dim.4.docs_ref, f32[2,2048]{1,0:T(2,128)} %ngain_ref.1, bf16[2,512,256]{2,1,0:T(8,128)(2,1)} %qw_ref.1, bf16[2,512,256]{2,1,0:T(8,128)(2,1)} %kw_ref.1, bf16[2,512,256]{2,1,0:T(8,128)(2,1)} %vw_ref.1, ...), custom_call_target="tpu_custom_call" | custom-call | tf_op jit(solution)/shard_map/fused_layers/pallas_call | solution.py:685
  105.6 2.3 %copy.12 = bf16[256,2048]{1,0:T(8,128)(2,1)} copy(bf16[256,2048]{1,0:T(8,128)(2,1)} %fused_layers.1) | data formatting | bytes 2097152
  (1 shorter events, 0.0 us)
Async XLA Ops:
  0.0 0.8 copy-start.1
  0.8 0.7 copy-start

commit v2 on v1

v2 whole, which is shorter than its diff:
```python
import functools

import jax
import jax.numpy as jnp
from jax import lax
from jax.experimental import pallas as pl
from jax.experimental.pallas import tpu as pltpu
from jax.sharding import PartitionSpec as P

SEG = 64
LEFT = 8
MAXREL = 256
LAYERS = 2


epsilon = 1e-06


def shifted(value, axis, steps):
    count = lax.axis_size(axis)
    initial, last = (max(0, -steps), min(count, count - steps))
    return lax.ppermute(value, axis, [(source, source + steps) for source in range(initial, last)])


def row_norm(values, gain):
    return values * lax.rsqrt(jnp.mean(values * values, axis=-1, keepdims=True) + epsilon) * gain


def bias_table(rel_bias):
    heads_here = rel_bias.shape[0]
    reach = LEFT * SEG
    width = (LEFT + 1) * SEG
    highest = reach + SEG - 1
    reversed_bias = rel_bias[:, ::-1]
    upper_fill = jnp.broadcast_to(rel_bias[:, -1:], (heads_here, highest - MAXREL))
    flat_row = jnp.concatenate([upper_fill, reversed_bias[:, : MAXREL + SEG]], axis=1)
    lines = [
        flat_row[:, SEG - 1 - position : SEG - 1 - position + width] for position in range(SEG)
    ]
    return jnp.stack(lines, axis=1)


def attend(query, ext_keys, ext_values, ext_docs, own_docs, offset, table):
    rows, heads_here, head_size = query.shape
    count = rows // SEG
    width = (LEFT + 1) * SEG
    blocks = query.reshape(count, SEG, heads_here, head_size)
    key_blocks = ext_keys.reshape(count + LEFT, SEG, heads_here, head_size)
    value_blocks = ext_values.reshape(count + LEFT, SEG, heads_here, head_size)
    doc_blocks = ext_docs.reshape(count + LEFT, SEG)
    score_parts = [
        jnp.einsum(
            "nqhd,nkhd->nhqk",
            blocks,
            key_blocks[earlier : earlier + count],
            preferred_element_type=jnp.float32,
        )
        for earlier in range(LEFT + 1)
    ]
    scores = jnp.concatenate(score_parts, axis=-1)
    scores = scores * head_size ** (-0.5) + table[None]
    doc_band = jnp.concatenate(
        [doc_blocks[earlier : earlier + count] for earlier in range(LEFT + 1)], axis=1
    )
    key_pos = (
        offset
        + SEG * jnp.arange(count, dtype=jnp.int32)[:, None]
        - LEFT * SEG
        + jnp.arange(width, dtype=jnp.int32)[None, :]
    )
    allowed = (key_pos >= 0)[:, None, None, :] & (
        doc_band[:, None, None, :] == own_docs.reshape(count, SEG)[:, None, :, None]
    )
    scores = jnp.where(allowed, scores, -1e30)
    peak = jnp.max(scores, axis=-1, keepdims=True)
    expo = jnp.exp(scores - peak)
    weights = (expo / jnp.sum(expo, axis=-1, keepdims=True)).astype(jnp.bfloat16)
    mixed = jnp.zeros((count, SEG, heads_here, head_size), jnp.float32)
    for earlier in range(LEFT + 1):
        part_weights = weights[..., earlier * SEG : (earlier + 1) * SEG]
        mixed = mixed + jnp.einsum(
            "nhqk,nkhd->nqhd",
            part_weights,
            value_blocks[earlier : earlier + count],
            preferred_element_type=jnp.float32,
        )
    return mixed.astype(jnp.bfloat16).reshape(rows, heads_here * head_size)


def on_device(
    stream,
    doc_ids,
    norm_gain,
    query_weight,
    key_weight,
    value_weight,
    out_weight,
    query_gain,
    key_gain,
    rel_bias,
):
    rows = stream.shape[0]
    heads_here = rel_bias.shape[0]
    head_size = query_gain.shape[1]
    local_width = heads_here * head_size
    reach = LEFT * SEG
    depth = -(-reach // rows)
    offset = lax.axis_index("sp") * rows
    col_width = out_weight.shape[2]
    col_start = lax.axis_index("tp") * col_width
    table = bias_table(rel_bias)
    x = stream
    for layer in range(LAYERS):
        widened = x.astype(jnp.float32)
        normed = row_norm(widened, norm_gain[layer]).astype(jnp.bfloat16)
        own_cols = normed
        q_raw = jnp.dot(
            own_cols,
            lax.all_gather(query_weight[layer], "sp", axis=0, tiled=True),
            preferred_element_type=jnp.float32,
        )
        k_raw = jnp.dot(
            normed,
            lax.all_gather(key_weight[layer], "sp", axis=0, tiled=True),
            preferred_element_type=jnp.float32,
        )
        v_raw = jnp.dot(
            normed,
            lax.all_gather(value_weight[layer], "sp", axis=0, tiled=True),
            preferred_element_type=jnp.float32,
        )
        query = row_norm(q_raw.reshape(rows, heads_here, head_size), query_gain[layer]).astype(
            jnp.bfloat16
        )
        keys = row_norm(
            k_raw.reshape(normed.shape[0], heads_here, head_size), key_gain[layer]
        ).astype(jnp.bfloat16)
        values = v_raw.astype(jnp.bfloat16)
        flat_keys = keys.reshape(rows, local_width)
        tail = (flat_keys, values, doc_ids)
        received = [
            shifted((tail[0], tail[1], tail[2]), "sp", distance_back)
            for distance_back in range(depth, 0, -1)
        ]
        ext_keys = jnp.concatenate([item[0] for item in received] + [flat_keys], axis=0)
        ext_values = jnp.concatenate([item[1] for item in received] + [values], axis=0)
        ext_docs = jnp.concatenate([item[2] for item in received] + [doc_ids], axis=0)
        ext_keys = ext_keys.reshape(reach + rows, heads_here, head_size)
        ext_values = ext_values.reshape(reach + rows, heads_here, head_size)
        attended = attend(query, ext_keys, ext_values, ext_docs, doc_ids, offset, table)
        all_heads = lax.all_gather(attended, "tp", axis=1, tiled=True)
        projected = jnp.dot(
            all_heads,
            lax.all_gather(out_weight[layer], "sp", axis=0, tiled=True),
            preferred_element_type=jnp.float32,
        )
        own_cols = lax.dynamic_slice_in_dim(widened, col_start, col_width, 1)
        new_cols = (own_cols + projected).astype(jnp.bfloat16)
        x = lax.all_gather(new_cols, "tp", axis=1, tiled=True)
    return x


MESH = pl.DeviceIdType.MESH
NEG = -1e30


def fused_kernel(
    sizes,
    x_in,
    docs_ref,
    ngain_ref,
    qw_in,
    kw_in,
    vw_in,
    wo_in,
    qgain_ref,
    kgain_ref,
    bias_ref,
    out_ref,
    x_ref,
    qw_ref,
    kw_ref,
    vw_ref,
    woin_ref,
    load,
    wt_ref,
    xg,
    wq,
    wo,
    docs,
    dcol,
    mids,
    ag,
    fin,
    bias,
    nb,
    q_s,
    k_s,
    v_s,
    o_s,
    doc_send,
    doc_recv,
    xz_send,
    xz_recv,
    xt_send,
    xt_recv,
    wz_send,
    wz_recv,
    wy_send,
    wy_recv,
    oz_send,
    oz_recv,
    ox_send,
    ox_recv,
    oy_send,
    oy_recv,
    op_send,
    op_recv,
    mz_send,
    mz_recv,
    mx_send,
    mx_recv,
    mc_send,
    mc_recv,
    nc_send,
    nc_recv,
    rs_send,
    rs_recv,
    az_send,
    az_recv,
    at_send,
    at_recv,
    fn_send,
    fn_recv,
):
    groups, seqs, tps = sizes
    rows, width = x_ref.shape
    cols = width // tps
    head = qgain_ref.shape[1]
    layers = wt_ref.shape[0]
    depth = bias.shape[1] - 1
    parts = xz_send.shape[1]
    tall = rows // parts
    pair = bias.shape[0]
    grp = lax.axis_index("grp")
    s = lax.axis_index("sp")
    t = lax.axis_index("tp")
    other_grp = 1 - grp
    core = t + 1 - 2 * lax.rem(t, 2)
    side = lax.rem(t + 2, tps)
    inner = (s > 0) & (s < seqs - 1)
    near = jnp.clip(s, 1, seqs - 2)
    far = seqs - 1 - near
    first = jnp.where(inner, seqs - 1 - s, near)
    inside = near - 1
    edge = jnp.where(near == 1, 0, seqs - 1)
    beyond = seqs - 1 - edge
    started = []

    def remote(src, dst, sems, out_index, in_index, where):
        return pltpu.make_async_remote_copy(
            src_ref=src,
            dst_ref=dst,
            send_sem=sems[0].at[out_index],
            recv_sem=sems[1].at[in_index],
            device_id=where,
            device_id_type=MESH,
        )

    def send(src, dst, sems, index, where):
        copy = remote(src, dst, sems, index, index, where)
        copy.start()
        started.append(copy)
        return copy

    def settle():
        for copy in started:
            copy.wait_send()
        started.clear()

    def ahead(o):
        return lax.rem(s + o, seqs)

    def block_rows(i):
        return pl.ds(pl.multiple_of(i * rows, rows), rows)

    def cut_rows(i, h):
        return pl.ds(pl.multiple_of(i * rows + h * tall, tall), tall)

    loads = [
        pltpu.make_async_copy(src, dst, load.at[n])
        for n, (src, dst) in enumerate(
            zip((x_in, qw_in, kw_in, vw_in, wo_in), (x_ref, qw_ref, kw_ref, vw_ref, woin_ref))
        )
    ]
    for copy in loads:
        copy.start()
    barrier = pltpu.get_barrier_semaphore()
    partners = [{"sp": ahead(o)} for o in range(1, seqs)]
    partners += [{"tp": core}, {"tp": side}, {"grp": other_grp}]
    for where in partners:
        pl.semaphore_signal(barrier, inc=1, device_id=where, device_id_type=MESH)
    pl.semaphore_wait(barrier, len(partners))
    loads[0].wait()

    own_cols = pl.ds(pl.multiple_of(t * cols, cols), cols)
    ohalf = woin_ref.shape[1] // 2
    opart = pl.ds(pl.multiple_of(grp * ohalf, ohalf), ohalf)
    hops = list(range(1, seqs))

    def x_copy(source, dest, h):
        place = xg.at[0, t, cut_rows(source, h), :]
        return remote(
            x_ref.at[h * tall : (h + 1) * tall, own_cols],
            place,
            (xz_send, xz_recv),
            (dest, h),
            (source, h),
            {"sp": dest},
        )

    def w_copy(layer, source, dest):
        return remote(
            wt_ref.at[layer, pair * (dest - 1) + grp],
            wq.at[layer, source, grp],
            (wz_send, wz_recv),
            (layer, dest),
            (layer, source),
            {"sp": dest},
        )

    def o_copy(layer, source, dest):
        return remote(
            woin_ref.at[layer, opart, :],
            wo.at[layer, t, source, opart, :],
            (oz_send, oz_recv),
            (layer, dest),
            (layer, source),
            {"sp": dest},
        )

    def w_near(layer, source):
        return remote(
            wt_ref.at[layer, pl.ds(pair * inside, pair)],
            wq.at[layer, source],
            (wz_send, wz_recv),
            (layer, near),
            (layer, source),
            {"sp": near},
        )

    def o_near(layer, source):
        return remote(
            woin_ref.at[layer],
            wo.at[layer, t, source],
            (oz_send, oz_recv),
            (layer, near),
            (layer, source),
            {"sp": near},
        )

    def outer_plan(n):
        if n == 0:
            return [x_copy(s, near, h) for h in range(parts)]
        if n == 1:
            x_far = [x_copy(s, far, h) for h in range(parts)]
            return [w_copy(0, s, near), x_far[0], w_copy(0, s, far)] + x_far[1:]
        if n == 2:
            return [o_copy(0, s, far), o_near(0, s)]
        plan = [w_copy(1, s, far), w_copy(1, s, near)]
        return plan + [o_copy(1, s, far), o_near(1, s), o_copy(1, s, seqs - 1 - s)]

    def inner_plan(n):
        other = seqs - 1 - s
        if n == 0:
            return [x_copy(s, other, h) for h in range(parts)]
        if n == 1:
            return [w_copy(0, s, other)]
        if n == 2:
            return [o_copy(0, s, other), w_copy(1, s, other)]
        return [o_copy(1, s, ahead(o)) for o in hops]

    def sends(plan, n, act):
        for copy in plan(n):
            getattr(copy, act)()

    def tp_copy(kind, block, h):
        held = side if kind == 2 else t
        place = xg.at[0, held, cut_rows(block, h), :]
        index = (kind, block, h)
        where = {"tp": side if kind == 1 else core}
        return remote(place, place, (xt_send, xt_recv), index, index, where)

    def w_relay(layer, block):
        place = wq.at[layer, block, grp]
        index = (layer, block)
        return remote(place, place, (wy_send, wy_recv), index, index, {"grp": other_grp})

    def o_relay(layer, kind, block):
        held = side if kind == 2 else t
        place = wo.at[layer, held, block, opart, :]
        sems = ((ox_send, ox_recv), (oy_send, oy_recv), (op_send, op_recv))[kind]
        index = (layer, block)
        where = {"tp": side} if kind == 0 else {"grp": other_grp}
        return remote(place, place, sems, index, index, where)

    def o_whole(layer):
        place = wo.at[layer, t, s]
        index = (layer, s)
        return remote(woin_ref.at[layer], place, (ox_send, ox_recv), index, index, {"tp": side})

    def begin(copy):
        copy.start()
        started.append(copy)

    def fan(block, h):
        x_copy(block, near, h).wait_recv()
        begin(tp_copy(1, block, h))
        begin(tp_copy(0, block, h))

    def pass_on(block, h):
        tp_copy(1, block, h).wait_recv()
        begin(tp_copy(2, block, h))

    def spread_w(layer, block):
        w_copy(layer, block, near).wait_recv()
        begin(w_relay(layer, block))

    def spread_o(layer, block, whole=False):
        (o_near(layer, block) if whole else o_copy(layer, block, near)).wait_recv()
        begin(o_relay(layer, 0, block))
        if not whole:
            begin(o_relay(layer, 1, block))

    def side_o(layer, block):
        o_relay(layer, 0, block).wait_recv()
        begin(o_relay(layer, 2, block))

    def ready_o(layer, relayed, sides):
        o_whole(layer).wait_recv()
        for block in relayed:
            o_relay(layer, 1, block).wait_recv()
        for block in sides:
            o_relay(layer, 2, block).wait_recv()

    def turn(layer):
        for which, source in enumerate((qw_ref, kw_ref, vw_ref)):
            turned = jnp.transpose(source[layer])
            for i in range(seqs):
                wt_ref[layer, i, which * head : (which + 1) * head, :] = turned[
                    i * head : (i + 1) * head, :
                ]

    @pl.when(inner)
    def _():
        sends(inner_plan, 0, "start")

    @pl.when(jnp.logical_not(inner))
    def _():
        sends(outer_plan, 0, "start")

    docs[s] = jnp.broadcast_to(docs_ref[...].astype(jnp.float32), docs.shape[1:])
    doc_c = [
        remote(docs.at[s], docs.at[s], (doc_send, doc_recv), o, o, {"sp": ahead(o)}) for o in hops
    ]
    for copy in doc_c:
        copy.start()
    for copy in loads[1:]:
        copy.wait()
    turn(0)

    @pl.when(inner)
    def _():
        sends(inner_plan, 1, "start")

    @pl.when(jnp.logical_not(inner))
    def _():
        for n in (1, 2):
            sends(outer_plan, n, "start")

    for layer in range(1, layers):
        turn(layer)

    @pl.when(jnp.logical_not(inner))
    def _():
        sends(outer_plan, 3, "start")

    for layer in range(layers):
        wo[layer, t, s] = woin_ref[layer]
    assert not started

    def project(layer, i):
        total = jnp.zeros((rows, 1), jnp.float32)
        for part in range(tps):
            piece = xg[layer, part, block_rows(i), :].astype(jnp.float32)
            total = total + jnp.sum(piece * piece, axis=1, keepdims=True)
        factor = lax.rsqrt(total * (1.0 / width) + epsilon)
        for part in range(tps):
            piece = xg[layer, part, block_rows(i), :].astype(jnp.float32)
            gain = ngain_ref[layer : layer + 1, part * cols : (part + 1) * cols]
            nb[:, part * cols : (part + 1) * cols] = (piece * factor * gain).astype(jnp.bfloat16)
        span = width // seqs
        raw = jnp.zeros((pair * 3 * head, rows), jnp.float32)
        for part in range(seqs):
            raw = raw + lax.dot_general(
                wq[layer, part].reshape(pair * 3 * head, span),
                nb[:, part * span : (part + 1) * span],
                (((1,), (1,)), ((), ())),
                preferred_element_type=jnp.float32,
            )

        def normal(value, gain):
            mean = jnp.mean(value * value, axis=0, keepdims=True)
            column = jnp.transpose(jnp.broadcast_to(gain, (128, head)))[:, 0:1]
            return value * lax.rsqrt(mean + epsilon) * column

        for a in range(pair):
            query, keys, values = [
                raw[(3 * a + n) * head : (3 * a + n + 1) * head] for n in range(3)
            ]
            query = normal(query, qgain_ref[layer : layer + 1, :]) * head ** (-0.5)
            keys = normal(keys, kgain_ref[layer : layer + 1, :])
            q_s[a, i] = query.astype(jnp.bfloat16)
            k_s[a, i] = jnp.transpose(keys).astype(jnp.bfloat16)
            v_s[a, i] = values.astype(jnp.bfloat16)

    def attend_block(j, a):
        pieces = []
        for i in range(max(0, j - depth), j + 1):
            score = jnp.dot(k_s[a, i], q_s[a, j], preferred_element_type=jnp.float32)
            same = dcol[i][:, 0:1] == docs[j, 0:1, :]
            pieces.append((i, jnp.where(same, score + bias[a, j - i], NEG)))
        peak = pieces[0][1].max(axis=0, keepdims=True)
        for _, piece in pieces[1:]:
            peak = jnp.maximum(peak, piece.max(axis=0, keepdims=True))
        mass = jnp.zeros((1, rows), jnp.float32)
        mixed = jnp.zeros((head, rows), jnp.float32)
        for i, piece in pieces:
            expo = jnp.exp(piece - peak)
            mass = mass + jnp.sum(expo, axis=0, keepdims=True)
            mixed = mixed + jnp.dot(
                v_s[a, i], expo.astype(jnp.bfloat16), preferred_element_type=jnp.float32
            )
        return (mixed / mass).astype(jnp.bfloat16)

    def out_product(layer, heads_all, held):
        return lax.dot_general(
            heads_all,
            wo[layer, held].reshape(-1, cols),
            (((0,), (0,)), ((), ())),
            preferred_element_type=jnp.float32,
        )

    def rest_copy(half, held):
        place = xg.at[1, held, block_rows(edge), :]
        return remote(place, place, (rs_send, rs_recv), half, half, {"sp": edge})

    def last_copy(j):
        return remote(
            o_s.at[j], ag.at[t, inside], (az_send, az_recv), j, inside, {"sp": j}
        )

    @pl.when(inner)
    def _():
        other = seqs - 1 - s
        for part in range(tps):
            xg[0, part, block_rows(s), :] = x_ref[:, part * cols : (part + 1) * cols]
        for layer in range(layers):
            wq[layer, s] = wt_ref[layer, pl.ds(pair * inside, pair)]
        begin(o_whole(0))
        key_seg = lax.broadcasted_iota(jnp.int32, (rows, rows), 0) // SEG
        query_seg = lax.broadcasted_iota(jnp.int32, (rows, rows), 1) // SEG
        entries = (bias_ref.shape[1] - 1) // 128 * 128
        tables = []
        for a in range(pair):
            line = bias_ref[pl.ds(pair * inside + a, 1), :]
            line, final = line[:, :entries], line[:, entries:]
            tables.append(
                jnp.concatenate(
                    [line, jnp.broadcast_to(final, (1, (depth + 2) * rows - entries))], axis=1
                )
            )
        for d in range(depth + 1):
            gap = query_seg + (d * rows) // SEG - key_seg
            for a in range(pair):
                spread = jnp.broadcast_to(
                    tables[a][:, d * rows : (d + 2) * rows], (rows, 2 * rows)
                )
                rolled = pltpu.roll(spread, 0, 1, stride=1, stride_axis=0)
                bias[a, d] = jnp.where((gap >= 0) & (gap <= LEFT), rolled[:, rows:], NEG)
        order = [(block, h) for h in range(parts) for block in (edge, other)]
        fan(*order[0])
        fan(*order[1])
        for copy in doc_c:
            copy.wait_recv()
        for i in range(seqs):
            dcol[i] = jnp.transpose(jnp.broadcast_to(docs[i, 0:1, :], (128, rows)))
        pass_on(*order[0])
        fan(*order[2])
        fan(*order[3])
        pass_on(*order[1])
        spread_w(0, edge)
        spread_w(0, other)
        pass_on(*order[2])
        fan(beyond, 0)
        pass_on(*order[3])
        spread_w(0, beyond)
        sends(inner_plan, 2, "start")
        for h in range(1, parts):
            fan(beyond, h)
        pass_on(beyond, 0)
        for h in range(1, parts):
            pass_on(beyond, h)
        for block in (edge, other, beyond):
            w_relay(0, block).wait_recv()
        project(0, s)
        spread_o(0, other)
        for block in (edge, other, beyond):
            for h in range(parts):
                tp_copy(0, block, h).wait_recv()
                tp_copy(2, block, h).wait_recv()
            project(0, block)
            if block is edge:
                spread_o(0, edge, True)
            if block is other:
                spread_o(0, beyond)

        mid_z, mid_x, mid_c, new_c = {}, {}, {}, {}
        turns = (0, 3, 1, 2)
        for n, j in enumerate(turns):
            for a in range(pair):
                mids[j, t, inside, a * head : (a + 1) * head, :] = attend_block(j, a)
            place = mids.at[j, t, inside]
            mid_z[j] = send(place, place, (mz_send, mz_recv), j, {"sp": other})
            mid_x[j, 0] = send(place, place, (mx_send, mx_recv), (j, 0), {"tp": side})
            if n == 0:
                side_o(0, other)
            if n == 1:
                side_o(0, edge)
            if n == 2:
                spread_w(1, other)

        def mid_first(j):
            mid_z[j].wait_recv()
            place = mids.at[j, t, 1 - inside]
            mid_x[j, 1] = send(place, place, (mx_send, mx_recv), (j, 1), {"tp": side})
            place = mids.at[j, t]
            mid_c[j, 0] = send(place, place, (mc_send, mc_recv), (j, 0), {"tp": core})

        def mid_second(j):
            for n in range(2):
                mid_x[j, n].wait_recv()
            place = mids.at[j, side]
            mid_c[j, 1] = send(place, place, (mc_send, mc_recv), (j, 1), {"tp": core})

        def mid_third(j):
            for half in range(2):
                mid_c[j, half].wait_recv()
            heads_all = mids[j].reshape(tps * seqs * head, rows)
            for half, held in enumerate((t, side)):
                kept = xg[0, held, block_rows(j), :].astype(jnp.float32)
                place = xg.at[1, held, block_rows(j), :]
                place[...] = (kept + out_product(0, heads_all, held)).astype(jnp.bfloat16)
                new_c[j, half] = send(place, place, (nc_send, nc_recv), (j, half), {"tp": core})
                if j in (0, seqs - 1):

                    @pl.when(edge == j)
                    def _(half=half, held=held):
                        rest_copy(half, held).start()

        def mid_fourth(j):
            for half in range(2):
                new_c[j, half].wait_recv()
            project(1, j)

        mid_first(0)
        side_o(0, beyond)
        mid_first(3)
        mid_second(0)
        spread_w(1, beyond)
        mid_first(1)
        mid_second(3)
        mid_first(2)
        mid_second(1)
        mid_second(2)
        spread_w(1, edge)
        begin(o_whole(1))
        sends(inner_plan, 3, "start")
        ready_o(0, (other, beyond), (edge, other, beyond))
        mid_third(0)
        mid_third(3)
        spread_o(1, beyond)
        mid_third(1)
        w_relay(1, edge).wait_recv()
        for block in (other, beyond):
            w_relay(1, block).wait_recv()
        mid_fourth(0)
        spread_o(1, other)
        mid_third(2)
        mid_fourth(3)
        spread_o(1, edge, True)
        side_o(1, beyond)
        mid_fourth(1)
        side_o(1, other)
        mid_fourth(2)
        for n, j in enumerate((0, seqs - 1, 1, 2)):
            for a in range(pair):
                o_s[j, a * head : (a + 1) * head, :] = attend_block(j, a)

            @pl.when(s != j)
            def _(j=j):
                last_copy(j).start()

            if n == 0:
                side_o(1, edge)
        ag[t, inside] = o_s[s]
        ag_in = remote(o_s.at[0], ag.at[t, 1 - inside], (az_send, az_recv), s, 1 - inside, {"sp": other})
        ag_in.wait_recv()
        ready_o(1, (other, beyond), (edge, other, beyond))
        for half, held in enumerate((t, side)):
            rest_copy(half, held).wait_send()
        for o in hops:
            last_copy(ahead(o)).wait_send()
        for n in range(4):
            sends(inner_plan, n, "wait_send")
        settle()

    @pl.when(jnp.logical_not(inner))
    def _():
        begin(o_whole(1))
        for copy in doc_c:
            copy.wait_recv()
        for block in (near, far, seqs - 1 - s):
            spread_o(1, block)
        for o in hops:
            side_o(1, ahead(o))
        for half, held in enumerate((t, side)):
            rest_copy(half, held).wait_recv()
        for n in range(2):
            place = ag.at[t, n]
            remote(place, place, (az_send, az_recv), s, n, {"sp": near}).wait_recv()
        ready_o(1, [ahead(o) for o in hops], [ahead(o) for o in hops])
        settle()
        for n in range(4):
            sends(outer_plan, n, "wait_send")

    block = ag.at[t]
    across = send(block, block, (at_send, at_recv), 0, {"tp": side})
    beside = send(block, block, (at_send, at_recv), 1, {"tp": core})
    across.wait_recv()
    block = ag.at[side]
    corner = send(block, block, (at_send, at_recv), 2, {"tp": core})
    beside.wait_recv()
    corner.wait_recv()
    heads_all = ag[...].reshape(tps * seqs * head, rows)
    last = []
    for half, held in enumerate((t, side)):
        kept = xg[1, held, block_rows(s), :].astype(jnp.float32)
        fin[held] = (kept + out_product(1, heads_all, held)).astype(jnp.bfloat16)
        place = fin.at[held]
        last.append(send(place, place, (fn_send, fn_recv), half, {"tp": core}))
    for copy in last:
        copy.wait_recv()
    for part in range(tps):
        out_ref[:, part * cols : (part + 1) * cols] = fin[part]
    settle()
    for copy in doc_c:
        copy.wait_send()

def fused_device(
    sizes,
    stream,
    doc_ids,
    norm_gain,
    query_weight,
    key_weight,
    value_weight,
    out_weight,
    query_gain,
    key_gain,
    rel_bias,
):
    groups, seqs, tps = sizes
    rows, width = stream.shape
    cols = width // tps
    layers, deep, _ = query_weight.shape
    head = query_gain.shape[1]
    depth = -(-LEFT * SEG // rows)

    dma = pltpu.SemaphoreType.DMA
    bf16 = jnp.bfloat16
    pair = seqs // 2
    whole = [stream, query_weight, key_weight, value_weight, out_weight]
    scratch = [pltpu.VMEM(one.shape, one.dtype) for one in whole] + [dma((len(whole),))]
    scratch += [
        pltpu.VMEM((layers, seqs, 3 * head, deep), bf16),
        pltpu.VMEM((layers, tps, seqs * rows, cols), bf16),
        pltpu.VMEM((layers, seqs, pair, 3 * head, deep), bf16),
        pltpu.VMEM((layers, tps, seqs) + out_weight.shape[1:], bf16),
        pltpu.VMEM((seqs, 8, rows), jnp.float32),
        pltpu.VMEM((seqs, rows, 128), jnp.float32),
        pltpu.VMEM((seqs, tps, 2, pair * head, rows), bf16),
        pltpu.VMEM((tps, 2, pair * head, rows), bf16),
        pltpu.VMEM((tps, rows, cols), bf16),
        pltpu.VMEM((pair, depth + 1, rows, rows), jnp.float32),
        pltpu.VMEM((rows, width), bf16),
        pltpu.VMEM((pair, seqs, head, rows), bf16),
        pltpu.VMEM((pair, seqs, rows, head), bf16),
        pltpu.VMEM((pair, seqs, head, rows), bf16),
        pltpu.VMEM((seqs, pair * head, rows), bf16),
    ]
    pairs = [
        (seqs,),
        (seqs, 2),
        (3, seqs, 2),
        (layers, seqs),
        (layers, seqs),
        (layers, seqs),
        (layers, seqs),
        (layers, seqs),
        (layers, seqs),
        (seqs,),
        (seqs, 2),
        (seqs, 2),
        (seqs, 2),
        (2,),
        (seqs,),
        (3,),
        (2,),
    ]
    scratch += [dma(shape) for shape in pairs for _ in range(2)]
    return pl.pallas_call(
        functools.partial(fused_kernel, sizes),
        name="fused_layers",
        out_shape=jax.ShapeDtypeStruct((rows, width), bf16),
        in_specs=[
            pl.BlockSpec(memory_space=pltpu.HBM if n in (0, 3, 4, 5, 6) else pltpu.VMEM)
            for n in range(10)
        ],
        out_specs=pl.BlockSpec(memory_space=pltpu.VMEM),
        scratch_shapes=scratch,
        compiler_params=pltpu.CompilerParams(
            collective_id=0, has_side_effects=True, vmem_limit_bytes=58 * 1024 * 1024
        ),
    )(
        stream,
        doc_ids[None],
        norm_gain,
        query_weight,
        key_weight,
        value_weight,
        out_weight,
        query_gain,
        key_gain,
        rel_bias,
    )


def solution(mesh):
    placed = (
        P(("grp", "sp"), None),
        P(("grp", "sp")),
        P(),
        P(None, "sp", "tp"),
        P(None, "sp", "tp"),
        P(None, "sp", "tp"),
        P(None, "sp", "tp"),
        P(),
        P(),
        P("tp", None),
    )
    sizes = tuple(mesh.shape[axis] for axis in ("grp", "sp", "tp"))

    def body(*args):
        one_head_each = args[-1].shape[0] == sizes[1]
        fits = sizes == (2, 4, 4) and args[0].shape[0] == MAXREL
        if one_head_each and fits:
            return fused_device(sizes, *args)
        return on_device(*args)

    return jax.shard_map(
        body, mesh=mesh, in_specs=placed, out_specs=P(("grp", "sp"), None), check_vma=False
    )
```

time: 108 us -> 91.7 us (0.85)
  Pallas kernels: 103 us -> 89.1 us
  local copies, waits for them, and re-layouts: 3.8 us -> 2.3 us
    pallas_call x1, Pallas kernels: 103 us -> 89.1 us  [fused_device(): pl.pallas_call(functools.partial(fused_kernel, sizes), name='fused_layers...]
    unnamed x5 -> x1, local copies, waits for them, and re-layouts: 2.33 us -> 2.3 us
where the time goes in v2:
time: 91.7 us; the launch traced here: 91.4 us
  Pallas kernels  89.1 us (97%)
  local copies, waits for them, and re-layouts  2.3 us (3%)
    pallas_call x1, Pallas kernels, fused_device(): pl.pallas_call(functools.partial(fused_kernel, sizes), name='fused_layers...  89.1 us
    unnamed x1, local copies, waits for them, and re-layouts  2.3 us

profile of v2, /device:TPU:0, one launch (start us, length us, event | category | flops | bytes accessed | tf_op | source)
XLA Modules:
  0.0 91.4 jit_solution(18135939309396572360)
XLA Ops:
  0.0 89.1 %fused_layers.1 = bf16[256,2048]{1,0:T(8,128)(2,1)} custom-call(bf16[256,2048]{1,0:T(8,128)(2,1)} %x_in.1, s32[1,256]{1,0:T(1,128)} %bitcast.1, f32[2,2048]{1,0:T(2,128)} %ngain_ref.1, bf16[2,512,256]{2,1,0:T(8,128)(2,1)} %qw_in.1, bf16[2,512,256]{2,1,0:T(8,128)(2,1)} %kw_in.1, bf16[2,512,256]{2,1,0:T(8,128)(2,1)} %vw_in.1, bf16[2,256,512]{2,1,0:T(8,128)(2,1)} %wo_in.1, ...), custom_call_target="tpu_custom_call" | custom-call | tf_op jit(solution)/shard_map/fused_layers/pallas_call | solution.py:832
  89.1 2.3 %copy.12 = bf16[256,2048]{1,0:T(8,128)(2,1)} copy(bf16[256,2048]{1,0:T(8,128)(2,1)} %fused_layers.1) | data formatting | bytes 2097152

commit v3 on v2

--- a/solution.py
+++ b/solution.py
@@ -339,24 +339,24 @@
             {"sp": dest},
         )
 
-    def w_near(layer, source):
+    def w_full(layer, source, dest):
         return remote(
-            wt_ref.at[layer, pl.ds(pair * inside, pair)],
+            wt_ref.at[layer, pl.ds(pair * (dest - 1), pair)],
             wq.at[layer, source],
             (wz_send, wz_recv),
-            (layer, near),
+            (layer, dest),
             (layer, source),
-            {"sp": near},
-        )
-
-    def o_near(layer, source):
+            {"sp": dest},
+        )
+
+    def o_full(layer, source, dest):
         return remote(
             woin_ref.at[layer],
             wo.at[layer, t, source],
             (oz_send, oz_recv),
-            (layer, near),
+            (layer, dest),
             (layer, source),
-            {"sp": near},
+            {"sp": dest},
         )
 
     def outer_plan(n):
@@ -364,21 +364,21 @@
             return [x_copy(s, near, h) for h in range(parts)]
         if n == 1:
             x_far = [x_copy(s, far, h) for h in range(parts)]
-            return [w_copy(0, s, near), x_far[0], w_copy(0, s, far)] + x_far[1:]
+            return [w_copy(0, s, near)] + x_far + [w_copy(0, s, far)]
         if n == 2:
-            return [o_copy(0, s, far), o_near(0, s)]
-        plan = [w_copy(1, s, far), w_copy(1, s, near)]
-        return plan + [o_copy(1, s, far), o_near(1, s), o_copy(1, s, seqs - 1 - s)]
+            return [o_copy(0, s, far), o_full(0, s, near)]
+        plan = [w_copy(1, s, near), w_copy(1, s, far)]
+        return plan + [o_copy(1, s, far), o_full(1, s, near), o_copy(1, s, seqs - 1 - s)]
 
     def inner_plan(n):
         other = seqs - 1 - s
         if n == 0:
             return [x_copy(s, other, h) for h in range(parts)]
         if n == 1:
-            return [w_copy(0, s, other)]
+            return [w_copy(0, s, other), o_full(1, s, edge)]
         if n == 2:
             return [o_copy(0, s, other), w_copy(1, s, other)]
-        return [o_copy(1, s, ahead(o)) for o in hops]
+        return [o_copy(1, s, other), o_copy(1, s, beyond)]
 
     def sends(plan, n, act):
         for copy in plan(n):
@@ -427,7 +427,7 @@
         begin(w_relay(layer, block))
 
     def spread_o(layer, block, whole=False):
-        (o_near(layer, block) if whole else o_copy(layer, block, near)).wait_recv()
+        (o_full(layer, block, near) if whole else o_copy(layer, block, near)).wait_recv()
         begin(o_relay(layer, 0, block))
         if not whole:
             begin(o_relay(layer, 1, block))
@@ -554,6 +554,16 @@
     def rest_copy(half, held):
         place = xg.at[1, held, block_rows(edge), :]
         return remote(place, place, (rs_send, rs_recv), half, half, {"sp": edge})
+
+    def ag_copy(kind, n):
+        place = ag.at[side if kind else t, n]
+        index = (kind, n)
+        where = {"tp": core if kind else side}
+        return remote(place, place, (at_send, at_recv), index, index, where)
+
+    def beside_copy():
+        place = ag.at[t]
+        return remote(place, place, (at_send, at_recv), (2, 0), (2, 0), {"tp": core})
 
     def last_copy(j):
         return remote(
@@ -694,28 +704,34 @@
         w_relay(1, edge).wait_recv()
         for block in (other, beyond):
             w_relay(1, block).wait_recv()
+        def finish(j):
+            for a in range(pair):
+                o_s[j, a * head : (a + 1) * head, :] = attend_block(j, a)
+
+            @pl.when(s != j)
+            def _():
+                last_copy(j).start()
+
+        mid_third(2)
         mid_fourth(0)
+        finish(0)
         spread_o(1, other)
-        mid_third(2)
         mid_fourth(3)
         spread_o(1, edge, True)
         side_o(1, beyond)
         mid_fourth(1)
+        finish(1)
         side_o(1, other)
         mid_fourth(2)
-        for n, j in enumerate((0, seqs - 1, 1, 2)):
-            for a in range(pair):
-                o_s[j, a * head : (a + 1) * head, :] = attend_block(j, a)
-
-            @pl.when(s != j)
-            def _(j=j):
-                last_copy(j).start()
-
-            if n == 0:
-                side_o(1, edge)
+        finish(3)
+        side_o(1, edge)
+        finish(2)
         ag[t, inside] = o_s[s]
+        begin(ag_copy(0, inside))
         ag_in = remote(o_s.at[0], ag.at[t, 1 - inside], (az_send, az_recv), s, 1 - inside, {"sp": other})
         ag_in.wait_recv()
+        begin(ag_copy(0, 1 - inside))
+        begin(beside_copy())
         ready_o(1, (other, beyond), (edge, other, beyond))
         for half, held in enumerate((t, side)):
             rest_copy(half, held).wait_send()
@@ -730,28 +746,29 @@
         begin(o_whole(1))
         for copy in doc_c:
             copy.wait_recv()
-        for block in (near, far, seqs - 1 - s):
+        spread_o(1, near, True)
+        for block in (seqs - 1 - s, far):
             spread_o(1, block)
         for o in hops:
             side_o(1, ahead(o))
         for half, held in enumerate((t, side)):
             rest_copy(half, held).wait_recv()
-        for n in range(2):
+        for n in (inside, 1 - inside):
             place = ag.at[t, n]
             remote(place, place, (az_send, az_recv), s, n, {"sp": near}).wait_recv()
-        ready_o(1, [ahead(o) for o in hops], [ahead(o) for o in hops])
+            begin(ag_copy(0, n))
+        begin(beside_copy())
+        ready_o(1, (far, seqs - 1 - s), (near, far, seqs - 1 - s))
         settle()
         for n in range(4):
             sends(outer_plan, n, "wait_send")
 
-    block = ag.at[t]
-    across = send(block, block, (at_send, at_recv), 0, {"tp": side})
-    beside = send(block, block, (at_send, at_recv), 1, {"tp": core})
-    across.wait_recv()
-    block = ag.at[side]
-    corner = send(block, block, (at_send, at_recv), 2, {"tp": core})
-    beside.wait_recv()
-    corner.wait_recv()
+    for n in (inside, 1 - inside):
+        ag_copy(0, n).wait_recv()
+        begin(ag_copy(1, n))
+    beside_copy().wait_recv()
+    for n in (inside, 1 - inside):
+        ag_copy(1, n).wait_recv()
     heads_all = ag[...].reshape(tps * seqs * head, rows)
     last = []
     for half, held in enumerate((t, side)):
@@ -825,7 +842,7 @@
         (seqs, 2),
         (2,),
         (seqs,),
-        (3,),
+        (3, 2),
         (2,),
     ]
     scratch += [dma(shape) for shape in pairs for _ in range(2)]

time: 91.7 us -> 88.3 us (0.963)
  the two profiles are of different devices: /device:TPU:0 before, /device:TPU:17 now
where the time goes in v3:
time: 88.3 us; the launch traced here: 88 us
  Pallas kernels  85.7 us (97%)
  local copies, waits for them, and re-layouts  2.3 us (3%)
    pallas_call x1, Pallas kernels, fused_device(): pl.pallas_call(functools.partial(fused_kernel, sizes), name='fused_layers...  85.7 us
    unnamed x1, local copies, waits for them, and re-layouts  2.3 us

profile of v3, /device:TPU:17, one launch (start us, length us, event | category | flops | bytes accessed | tf_op | source)
XLA Modules:
  0.0 88.0 jit_solution(4652664933265581545)
XLA Ops:
  0.0 85.7 %fused_layers.1 = bf16[256,2048]{1,0:T(8,128)(2,1)} custom-call(bf16[256,2048]{1,0:T(8,128)(2,1)} %x_in.1, s32[1,256]{1,0:T(1,128)} %bitcast.1, f32[2,2048]{1,0:T(2,128)} %ngain_ref.1, bf16[2,512,256]{2,1,0:T(8,128)(2,1)} %qw_in.1, bf16[2,512,256]{2,1,0:T(8,128)(2,1)} %kw_in.1, bf16[2,512,256]{2,1,0:T(8,128)(2,1)} %vw_in.1, bf16[2,256,512]{2,1,0:T(8,128)(2,1)} %wo_in.1, ...), custom_call_target="tpu_custom_call" | custom-call | tf_op jit(solution)/shard_map/fused_layers/pallas_call | solution.py:849
  85.7 2.3 %copy.12 = bf16[256,2048]{1,0:T(8,128)(2,1)} copy(bf16[256,2048]{1,0:T(8,128)(2,1)} %fused_layers.1) | data formatting | bytes 2097152

commit v4 on v3

--- a/solution.py
+++ b/solution.py
@@ -183,6 +183,7 @@
     vw_ref,
     woin_ref,
     load,
+    save,
     wt_ref,
     xg,
     wq,
@@ -193,6 +194,7 @@
     ag,
     fin,
     bias,
+    masked,
     nb,
     q_s,
     k_s,
@@ -436,12 +438,18 @@
         o_relay(layer, 0, block).wait_recv()
         begin(o_relay(layer, 2, block))
 
-    def ready_o(layer, relayed, sides):
-        o_whole(layer).wait_recv()
+    def ready_own(layer, relayed):
         for block in relayed:
             o_relay(layer, 1, block).wait_recv()
+
+    def ready_side(layer, sides):
+        o_whole(layer).wait_recv()
         for block in sides:
             o_relay(layer, 2, block).wait_recv()
+
+    def ready_o(layer, relayed, sides):
+        ready_own(layer, relayed)
+        ready_side(layer, sides)
 
     def turn(layer):
         for which, source in enumerate((qw_ref, kw_ref, vw_ref)):
@@ -524,12 +532,18 @@
             k_s[a, i] = jnp.transpose(keys).astype(jnp.bfloat16)
             v_s[a, i] = values.astype(jnp.bfloat16)
 
+    links = [(i, j) for j in range(seqs) for i in range(max(0, j - depth), j + 1)]
+
+    def mask(a):
+        for n, (i, j) in enumerate(links):
+            same = dcol[i][:, 0:1] == docs[j, 0:1, :]
+            masked[a, n] = jnp.where(same, bias[a, j - i], NEG)
+
     def attend_block(j, a):
         pieces = []
         for i in range(max(0, j - depth), j + 1):
             score = jnp.dot(k_s[a, i], q_s[a, j], preferred_element_type=jnp.float32)
-            same = dcol[i][:, 0:1] == docs[j, 0:1, :]
-            pieces.append((i, jnp.where(same, score + bias[a, j - i], NEG)))
+            pieces.append((i, score + masked[a, links.index((i, j))]))
         peak = pieces[0][1].max(axis=0, keepdims=True)
         for _, piece in pieces[1:]:
             peak = jnp.maximum(peak, piece.max(axis=0, keepdims=True))
@@ -605,12 +619,14 @@
             copy.wait_recv()
         for i in range(seqs):
             dcol[i] = jnp.transpose(jnp.broadcast_to(docs[i, 0:1, :], (128, rows)))
+        mask(0)
         pass_on(*order[0])
         fan(*order[2])
         fan(*order[3])
         pass_on(*order[1])
         spread_w(0, edge)
         spread_w(0, other)
+        mask(1)
         pass_on(*order[2])
         fan(beyond, 0)
         pass_on(*order[3])
@@ -663,20 +679,21 @@
             place = mids.at[j, side]
             mid_c[j, 1] = send(place, place, (mc_send, mc_recv), (j, 1), {"tp": core})
 
-        def mid_third(j):
-            for half in range(2):
-                mid_c[j, half].wait_recv()
+        def mid_third(j, half):
+            if half == 0:
+                for n in range(2):
+                    mid_c[j, n].wait_recv()
+            held = side if half else t
             heads_all = mids[j].reshape(tps * seqs * head, rows)
-            for half, held in enumerate((t, side)):
-                kept = xg[0, held, block_rows(j), :].astype(jnp.float32)
-                place = xg.at[1, held, block_rows(j), :]
-                place[...] = (kept + out_product(0, heads_all, held)).astype(jnp.bfloat16)
-                new_c[j, half] = send(place, place, (nc_send, nc_recv), (j, half), {"tp": core})
-                if j in (0, seqs - 1):
-
-                    @pl.when(edge == j)
-                    def _(half=half, held=held):
-                        rest_copy(half, held).start()
+            kept = xg[0, held, block_rows(j), :].astype(jnp.float32)
+            place = xg.at[1, held, block_rows(j), :]
+            place[...] = (kept + out_product(0, heads_all, held)).astype(jnp.bfloat16)
+            new_c[j, half] = send(place, place, (nc_send, nc_recv), (j, half), {"tp": core})
+            if j in (0, seqs - 1):
+
+                @pl.when(edge == j)
+                def _():
+                    rest_copy(half, held).start()
 
         def mid_fourth(j):
             for half in range(2):
@@ -696,11 +713,15 @@
         spread_w(1, edge)
         begin(o_whole(1))
         sends(inner_plan, 3, "start")
-        ready_o(0, (other, beyond), (edge, other, beyond))
-        mid_third(0)
-        mid_third(3)
+        ready_own(0, (other, beyond))
+        mid_third(0, 0)
+        mid_third(3, 0)
+        ready_side(0, (edge, other, beyond))
+        mid_third(0, 1)
+        mid_third(3, 1)
         spread_o(1, beyond)
-        mid_third(1)
+        mid_third(1, 0)
+        mid_third(1, 1)
         w_relay(1, edge).wait_recv()
         for block in (other, beyond):
             w_relay(1, block).wait_recv()
@@ -712,7 +733,8 @@
             def _():
                 last_copy(j).start()
 
-        mid_third(2)
+        mid_third(2, 0)
+        mid_third(2, 1)
         mid_fourth(0)
         finish(0)
         spread_o(1, other)
@@ -770,19 +792,28 @@
     for n in (inside, 1 - inside):
         ag_copy(1, n).wait_recv()
     heads_all = ag[...].reshape(tps * seqs * head, rows)
-    last = []
+    last, stores = [], []
+
+    def store(part):
+        place = out_ref.at[:, pl.ds(pl.multiple_of(part * cols, cols), cols)]
+        return pltpu.make_async_copy(fin.at[part], place, save.at[part])
+
     for half, held in enumerate((t, side)):
         kept = xg[1, held, block_rows(s), :].astype(jnp.float32)
         fin[held] = (kept + out_product(1, heads_all, held)).astype(jnp.bfloat16)
         place = fin.at[held]
         last.append(send(place, place, (fn_send, fn_recv), half, {"tp": core}))
-    for copy in last:
+        stores.append(store(held))
+        stores[-1].start()
+    for copy, held in zip(last, (core, lax.rem(core + 2, tps))):
         copy.wait_recv()
-    for part in range(tps):
-        out_ref[:, part * cols : (part + 1) * cols] = fin[part]
+        stores.append(store(held))
+        stores[-1].start()
     settle()
     for copy in doc_c:
         copy.wait_send()
+    for copy in stores:
+        copy.wait()
 
 def fused_device(
     sizes,
@@ -807,8 +838,9 @@
     dma = pltpu.SemaphoreType.DMA
     bf16 = jnp.bfloat16
     pair = seqs // 2
+    links = sum(min(j, depth) + 1 for j in range(seqs))
     whole = [stream, query_weight, key_weight, value_weight, out_weight]
-    scratch = [pltpu.VMEM(one.shape, one.dtype) for one in whole] + [dma((len(whole),))]
+    scratch = [pltpu.VMEM(one.shape, one.dtype) for one in whole] + [dma((len(whole),)), dma((tps,))]
     scratch += [
         pltpu.VMEM((layers, seqs, 3 * head, deep), bf16),
         pltpu.VMEM((layers, tps, seqs * rows, cols), bf16),
@@ -820,6 +852,7 @@
         pltpu.VMEM((tps, 2, pair * head, rows), bf16),
         pltpu.VMEM((tps, rows, cols), bf16),
         pltpu.VMEM((pair, depth + 1, rows, rows), jnp.float32),
+        pltpu.VMEM((pair, links, rows, rows), jnp.float32),
         pltpu.VMEM((rows, width), bf16),
         pltpu.VMEM((pair, seqs, head, rows), bf16),
         pltpu.VMEM((pair, seqs, rows, head), bf16),
@@ -854,7 +887,7 @@
             pl.BlockSpec(memory_space=pltpu.HBM if n in (0, 3, 4, 5, 6) else pltpu.VMEM)
             for n in range(10)
         ],
-        out_specs=pl.BlockSpec(memory_space=pltpu.VMEM),
+        out_specs=pl.BlockSpec(memory_space=pl.ANY),
         scratch_shapes=scratch,
         compiler_params=pltpu.CompilerParams(
             collective_id=0, has_side_effects=True, vmem_limit_bytes=58 * 1024 * 1024

time: 88.3 us -> 87.6 us (level)
  the two profiles are of different devices: /device:TPU:17 before, /device:TPU:0 now
where the time goes in v4:
time: 87.6 us; the launch traced here: 85.9 us
  Pallas kernels  83.6 us (95%)
  local copies, waits for them, and re-layouts  2.3 us (3%)
    pallas_call x1, Pallas kernels, fused_device(): pl.pallas_call(functools.partial(fused_kernel, sizes), name='fused_layers...  83.6 us
    unnamed x1, local copies, waits for them, and re-layouts  2.3 us

profile of v4, /device:TPU:0, one launch (start us, length us, event | category | flops | bytes accessed | tf_op | source)
XLA Modules:
  0.0 85.9 jit_solution(12007948758185778551)
XLA Ops:
  0.0 83.6 %fused_layers.1 = bf16[256,2048]{1,0:T(8,128)(2,1)} custom-call(bf16[256,2048]{1,0:T(8,128)(2,1)} %x_in.1, s32[1,256]{1,0:T(1,128)} %bitcast.1, f32[2,2048]{1,0:T(2,128)} %ngain_ref.1, bf16[2,512,256]{2,1,0:T(8,128)(2,1)} %qw_in.1, bf16[2,512,256]{2,1,0:T(8,128)(2,1)} %kw_in.1, bf16[2,512,256]{2,1,0:T(8,128)(2,1)} %vw_in.1, bf16[2,256,512]{2,1,0:T(8,128)(2,1)} %wo_in.1, ...), custom_call_target="tpu_custom_call" | custom-call | tf_op jit(solution)/shard_map/fused_layers/pallas_call | solution.py:882
  83.6 2.3 %copy.12 = bf16[256,2048]{1,0:T(8,128)(2,1)} copy(bf16[256,2048]{1,0:T(8,128)(2,1)} %fused_layers.1) | data formatting | bytes 2097152

commit v5 on v4

--- a/solution.py
+++ b/solution.py
@@ -716,11 +716,11 @@
         ready_own(0, (other, beyond))
         mid_third(0, 0)
         mid_third(3, 0)
+        mid_third(1, 0)
         ready_side(0, (edge, other, beyond))
         mid_third(0, 1)
         mid_third(3, 1)
         spread_o(1, beyond)
-        mid_third(1, 0)
         mid_third(1, 1)
         w_relay(1, edge).wait_recv()
         for block in (other, beyond):

time: 87.6 us -> 87.6 us (level)
  no operation moved by 1% of the time
where the time goes in v5:
time: 87.6 us; the launch traced here: 85.9 us
  Pallas kernels  83.6 us (95%)
  local copies, waits for them, and re-layouts  2.3 us (3%)
    pallas_call x1, Pallas kernels, fused_device(): pl.pallas_call(functools.partial(fused_kernel, sizes), name='fused_layers...  83.6 us
    unnamed x1, local copies, waits for them, and re-layouts  2.3 us

profile of v5, /device:TPU:0, one launch (start us, length us, event | category | flops | bytes accessed | tf_op | source)
XLA Modules:
  0.0 85.9 jit_solution(3649646189986467006)
XLA Ops:
  0.0 83.6 %fused_layers.1 = bf16[256,2048]{1,0:T(8,128)(2,1)} custom-call(bf16[256,2048]{1,0:T(8,128)(2,1)} %x_in.1, s32[1,256]{1,0:T(1,128)} %bitcast.1, f32[2,2048]{1,0:T(2,128)} %ngain_ref.1, bf16[2,512,256]{2,1,0:T(8,128)(2,1)} %qw_in.1, bf16[2,512,256]{2,1,0:T(8,128)(2,1)} %kw_in.1, bf16[2,512,256]{2,1,0:T(8,128)(2,1)} %vw_in.1, bf16[2,256,512]{2,1,0:T(8,128)(2,1)} %wo_in.1, ...), custom_call_target="tpu_custom_call" | custom-call | tf_op jit(solution)/shard_map/fused_layers/pallas_call | solution.py:882
  83.6 2.3 %copy.12 = bf16[256,2048]{1,0:T(8,128)(2,1)} copy(bf16[256,2048]{1,0:T(8,128)(2,1)} %fused_layers.1) | data formatting | bytes 2097152
